TPU v7x, 256 devices: a 4x2x16 block of a 4x16x16 slice. The times are simulated.
256 devices in a mesh: grp: 2 (over y), sp: 32 (over z, core), tp: 4 (over x).
Axes of the slice: x: 4, y: 2, z: 16, core: 2. Of those that a mesh axis runs over, the one named last changes fastest.
The devices are a block of a 4x16x16 slice.
Arguments:
- queries: bfloat16 [16384, 1024], P(('grp', 'sp'), 'tp'), parts along dimension 0, may hold values from -7 to 10
- keys: bfloat16 [16384, 1024], P(('grp', 'sp'), 'tp'), parts along dimension 0, may hold values from -14 to 7
- values: bfloat16 [16384, 1024], P(('grp', 'sp'), 'tp'), parts along dimension 0, may hold values from -6 to 6
- resid: bfloat16 [16384, 2048], P(('grp', 'sp', 'tp')), parts along dimension 0, may hold values from -18 to 18
- out_weight: bfloat16 [1024, 2048], P('tp'), may hold values from -0.375 to 0.375
- gate_weight: bfloat16 [2048, 3072], P('sp', 'tp'), may hold values from -0.125 to 0.125
- value_weight: bfloat16 [2048, 3072], P('sp', 'tp'), may hold values from -0.125 to 0.125
- conv_gate: float32 [3, 3072], P(None, 'tp'), may hold values from -3 to 3
- conv_value: float32 [3, 3072], P(None, 'tp'), may hold values from -3 to 3
- norm_gain: float32 [2048], replicated, may hold values from 0.1 to 1.9
- down_weight: bfloat16 [3072, 2048], P('tp', 'sp'), may hold values from -0.109375 to 0.109375
Outputs:
- layer_out: bfloat16 [16384, 2048], P(('grp', 'sp', 'tp')), parts along dimension 0
There are 2 independent parts, one for each index of `grp`. A program takes and returns all parts, laid end to end along the dimension named above; an argument that names none is the same for every part. Nothing has to cross between parts.
All inputs are finite; a program needn't handle non-finite values.
Results may differ from a plain program's by a relative error of at most 0.0058.
Values may be sent and summed in bfloat16 or wider, within the bound.
A program may use at most 128 MiB of HBM per device.

v0:
```python
import jax
import jax.numpy as jnp
from jax import lax
from jax.sharding import PartitionSpec as P

HEAD = 64


epsilon = 1e-06


def side_by_side(arrays, axis, dim, along):
    ends, at = ([], 0)
    for a in arrays[:-1]:
        at += a.shape[along]
        ends.append(at)
    both = jnp.concatenate(arrays, axis=along)
    return tuple(jnp.split(lax.all_gather(both, axis, axis=dim, tiled=True), ends, axis=along))


def cut_along(shard, dim, peers):
    dims = shard.shape
    pieces = shard.reshape(*dims[:dim], peers, dims[dim] // peers, *dims[dim + 1 :])
    return jnp.moveaxis(pieces, dim, 0)


def summed_on_arrival(shard, axis, dim):
    pieces = cut_along(shard, dim, lax.axis_size(axis))
    arrived = lax.all_to_all(pieces, axis, split_axis=0, concat_axis=0, tiled=True)
    return arrived.sum(axis=0)


def joined_along(pieces, dim):
    pieces = jnp.moveaxis(pieces, 0, dim)
    dims = pieces.shape
    return pieces.reshape(*dims[:dim], dims[dim] * dims[dim + 1], *dims[dim + 2 :])


def from_everyone(shard, axis):
    peers = lax.axis_size(axis)
    return lax.all_to_all(
        jnp.broadcast_to(shard[None], (peers, *shard.shape)), axis, 0, 0, tiled=True
    )


def gathered_copies(shard, axis, dim):
    return joined_along(from_everyone(shard, axis), dim)


def shifted(block, axis, distance):
    devices = range(lax.axis_size(axis))
    route = [(i - distance, i) for i in devices if i - distance in devices]
    return lax.ppermute(block, axis, route)


def block_terms(query_rows, key_rows, value_rows, query_place, key_place):
    scores = jnp.einsum(
        "qhe,khe->hqk", query_rows, key_rows, preferred_element_type=jnp.float32
    ) * HEAD ** (-0.5)
    causal = (key_place[None, :] < query_place[:, None])[None]
    stay_log = jnp.where(causal, jax.nn.log_sigmoid(-scores), 0.0)
    suffix = lax.cumsum(stay_log, axis=2, reverse=True) - stay_log
    local_weight = jnp.where(causal, jnp.exp(jax.nn.log_sigmoid(scores) + suffix), 0.0).astype(
        jnp.bfloat16
    )
    part = jnp.einsum("hqk,khe->hqe", local_weight, value_rows, preferred_element_type=jnp.float32)
    return (jnp.sum(stay_log, axis=2), part)


def normalize(state, norm_gain):
    values = state.astype(jnp.float32)
    scaled = values * lax.rsqrt(jnp.mean(values * values, axis=-1, keepdims=True) + epsilon)
    return (scaled * norm_gain).astype(jnp.bfloat16)


def causal_conv(rim_rows, rows, taps):
    extended = jnp.concatenate([rim_rows, rows], axis=0).astype(jnp.float32)
    length = rows.shape[0]
    total = jnp.zeros(rows.shape, jnp.float32)
    for start_displacement in range(taps.shape[0]):
        total = (
            total
            + taps[start_displacement] * extended[start_displacement : start_displacement + length]
        )
    return total


def body(
    queries,
    keys,
    values,
    resid,
    out_weight,
    gate_weight,
    value_weight,
    conv_gate,
    conv_value,
    norm_gain,
    down_weight,
):
    tok_dev = queries.shape[0]
    mix_local = queries.shape[1]
    head_count = mix_local // HEAD
    sp_count = lax.axis_size("sp")
    block = tok_dev * min(sp_count, max(1, 1024 // tok_dev))
    early_up = side_by_side((gate_weight, value_weight), "sp", 0, 1)
    early_down = lax.all_gather(down_weight, "sp", axis=1, tiled=True)
    paired = jnp.concatenate([keys, values], axis=1)
    gathered = lax.all_gather(paired, "sp", axis=0, tiled=True)
    mine = lax.axis_index("sp")
    query_place = mine * tok_dev + jnp.arange(tok_dev, dtype=jnp.int32)
    query_rows = queries.reshape(tok_dev, head_count, HEAD)

    def add_block(index, carry):
        start = index * block
        piece = lax.dynamic_slice_in_dim(gathered, start, block, 0)
        key_rows = piece[:, :mix_local].reshape(block, head_count, HEAD)
        value_rows = piece[:, mix_local:].reshape(block, head_count, HEAD)
        key_place = start + jnp.arange(block, dtype=jnp.int32)
        total, part = block_terms(query_rows, key_rows, value_rows, query_place, key_place)
        return carry * jnp.exp(total)[:, :, None] + part

    start_carry = jnp.zeros((head_count, tok_dev, HEAD), jnp.float32)
    attended = lax.fori_loop(0, mine * tok_dev // block + 1, add_block, start_carry)
    mixed = jnp.transpose(attended, (1, 0, 2)).reshape(tok_dev, mix_local).astype(jnp.bfloat16)
    projected = summed_on_arrival(
        jnp.dot(mixed, out_weight, preferred_element_type=jnp.float32), "tp", 0
    )
    state = (resid.astype(jnp.float32) + projected).astype(jnp.bfloat16)
    normed = gathered_copies(normalize(state, norm_gain), "tp", 0)
    ff_local = gate_weight.shape[1]
    gate_full = jnp.dot(normed, early_up[0], preferred_element_type=jnp.float32)
    value_full = jnp.dot(normed, early_up[1], preferred_element_type=jnp.float32)
    gate_pre = gate_full.astype(jnp.bfloat16)
    value_pre = value_full.astype(jnp.bfloat16)
    taps_count = conv_gate.shape[0]
    rim = jnp.concatenate(
        [gate_pre[tok_dev - taps_count + 1 :], value_pre[tok_dev - taps_count + 1 :]], axis=1
    )
    before = shifted(rim, "sp", 1)
    conv_gate_out = causal_conv(before[:, :ff_local], gate_pre, conv_gate)
    conv_value_out = causal_conv(before[:, ff_local:], value_pre, conv_value)
    gated = (jax.nn.silu(conv_gate_out) * conv_value_out).astype(jnp.bfloat16)
    partial_sum = jnp.dot(gated, early_down, preferred_element_type=jnp.float32)
    ffn_share = summed_on_arrival(partial_sum, "tp", 0)
    return (state.astype(jnp.float32) + ffn_share).astype(jnp.bfloat16)


def solution(mesh):
    placed = (
        P(("grp", "sp"), "tp"),
        P(("grp", "sp"), "tp"),
        P(("grp", "sp"), "tp"),
        P(("grp", "sp", "tp"), None),
        P("tp", None),
        P("sp", "tp"),
        P("sp", "tp"),
        P(None, "tp"),
        P(None, "tp"),
        P(),
        P("tp", "sp"),
    )
    return jax.shard_map(
        body, mesh=mesh, in_specs=placed, out_specs=P(("grp", "sp", "tp"), None), check_vma=False
    )
```

profile of v0, /device:TPU:1824, one launch (start us, length us, event | category | flops | bytes accessed | tf_op | source)
XLA Modules:
  0.0 450.8 jit_solution(10426871388544455303)
XLA Ops:
  13.1 85.2 %all-gather.4.cloned.1.call-done = bf16[8192,512]{0,1:T(8,128)(2,1)} async-done(((bf16[256,512]{0,1:T(8,128)(2,1)}), bf16[8192,512]{0,1:T(8,128)(2,1)}) %all-gather.4.cloned.1.call-update) | async-done | bytes 8388624 | tf_op jit(solution)/shard_map/all_gather | solution.py:109
  98.2 248.4 %while.11 = (s32[]{:T(128)}, f32[4,256,64]{1,2,0:T(8,128)S(1)}, s32[]{:T(128)}, bf16[8192,512]{0,1:T(8,128)(2,1)}, bf16[256,4,64]{0,2,1:T(8,128)(2,1)S(1)}, /*in...) while((s32[]{:T(128)}, f32[4,256,64]{1,2,0:T(8,128)S(1)}, ...), condition=%wide.region_4.5_spmd.clone, body=%wide.region_0.4_spmd.clone.sunk | while | flops 435617024 | bytes 84539640 | solution.py:124
  99.8 5.3 %fusion.70 = (f32[4,256]{1,0:T(4,128)S(1)}, f32[4,256,1024]{1,2,0:T(8,128)S(1)}, f32[4,1024,256]{2,1,0:T(8,128)}) fusion(pred[256,1024]{0,1:T(8,128)(4,1)S(1)} %broadcast_compare_fusion.2, bf16[1024,4,64]{0,2,1:T(8,128)(2,1)S(1)} %bitcast.73, bf16[256,4,64]{0,2,1:T(8,128)(2,1)S(1)} %get-tuple-element.163), kind=kOutput, calls=%fused_computation.27.clone.1 | convolution fusion | flops 144702464 | bytes 9310208 | tf_op jit(solution)/shard_map/while/body/qhe,khe->hqk/dot_general | solution.py:57
  105.1 10.1 %fusion.71 = f32[4,256,8,128]{1,2,3,0:T(8,128)S(1)} fusion(f32[4,256,8,128]{1,3,2,0:T(8,128)S(1)} %bitcast.71), kind=kOutput, calls=%fused_computation.18.clone.1 | output fusion | flops 133169152 | bytes 8388608 | tf_op jit(solution)/shard_map/reduce-window
  115.2 2.0 copy-done.1
  117.3 2.6 broadcast_add_fusion.2
  122.2 6.6 %fusion.72 = bf16[4,256,1024]{1,2,0:T(8,128)(2,1)S(1)} fusion(f32[4,256,8,128]{1,3,2,0:T(8,128)S(1)} %copy.35, f32[4,1024,256]{2,1,0:T(8,128)S(1)} %copy-done.2, pred[256,1024]{0,1:T(8,128)(4,1)S(1)} %broadcast_compare_fusion.2), kind=kLoop, calls=%fused_computation.9.clone.1 | loop fusion | flops 22020096 | bytes 10747904 | tf_op jit(solution)/shard_map/while/body/convert_element_type | solution.py:63
  130.9 5.3 %fusion.70 = (f32[4,256]{1,0:T(4,128)S(1)}, f32[4,256,1024]{1,2,0:T(8,128)S(1)}, f32[4,1024,256]{2,1,0:T(8,128)}) fusion(pred[256,1024]{0,1:T(8,128)(4,1)S(1)} %broadcast_compare_fusion.2, bf16[1024,4,64]{0,2,1:T(8,128)(2,1)S(1)} %bitcast.73, bf16[256,4,64]{0,2,1:T(8,128)(2,1)S(1)} %get-tuple-element.163), kind=kOutput, calls=%fused_computation.27.clone.1 | convolution fusion | flops 144702464 | bytes 9310208 | tf_op jit(solution)/shard_map/while/body/qhe,khe->hqk/dot_general | solution.py:57
  136.2 10.1 %fusion.71 = f32[4,256,8,128]{1,2,3,0:T(8,128)S(1)} fusion(f32[4,256,8,128]{1,3,2,0:T(8,128)S(1)} %bitcast.71), kind=kOutput, calls=%fused_computation.18.clone.1 | output fusion | flops 133169152 | bytes 8388608 | tf_op jit(solution)/shard_map/reduce-window
  146.3 2.0 copy-done.1
  148.4 2.6 broadcast_add_fusion.2
  153.3 6.6 %fusion.72 = bf16[4,256,1024]{1,2,0:T(8,128)(2,1)S(1)} fusion(f32[4,256,8,128]{1,3,2,0:T(8,128)S(1)} %copy.35, f32[4,1024,256]{2,1,0:T(8,128)S(1)} %copy-done.2, pred[256,1024]{0,1:T(8,128)(4,1)S(1)} %broadcast_compare_fusion.2), kind=kLoop, calls=%fused_computation.9.clone.1 | loop fusion | flops 22020096 | bytes 10747904 | tf_op jit(solution)/shard_map/while/body/convert_element_type | solution.py:63
  162.0 5.3 %fusion.70 = (f32[4,256]{1,0:T(4,128)S(1)}, f32[4,256,1024]{1,2,0:T(8,128)S(1)}, f32[4,1024,256]{2,1,0:T(8,128)}) fusion(pred[256,1024]{0,1:T(8,128)(4,1)S(1)} %broadcast_compare_fusion.2, bf16[1024,4,64]{0,2,1:T(8,128)(2,1)S(1)} %bitcast.73, bf16[256,4,64]{0,2,1:T(8,128)(2,1)S(1)} %get-tuple-element.163), kind=kOutput, calls=%fused_computation.27.clone.1 | convolution fusion | flops 144702464 | bytes 9310208 | tf_op jit(solution)/shard_map/while/body/qhe,khe->hqk/dot_general | solution.py:57
  167.3 10.1 %fusion.71 = f32[4,256,8,128]{1,2,3,0:T(8,128)S(1)} fusion(f32[4,256,8,128]{1,3,2,0:T(8,128)S(1)} %bitcast.71), kind=kOutput, calls=%fused_computation.18.clone.1 | output fusion | flops 133169152 | bytes 8388608 | tf_op jit(solution)/shard_map/reduce-window
  177.4 2.0 copy-done.1
  179.5 2.6 broadcast_add_fusion.2
  184.3 6.6 %fusion.72 = bf16[4,256,1024]{1,2,0:T(8,128)(2,1)S(1)} fusion(f32[4,256,8,128]{1,3,2,0:T(8,128)S(1)} %copy.35, f32[4,1024,256]{2,1,0:T(8,128)S(1)} %copy-done.2, pred[256,1024]{0,1:T(8,128)(4,1)S(1)} %broadcast_compare_fusion.2), kind=kLoop, calls=%fused_computation.9.clone.1 | loop fusion | flops 22020096 | bytes 10747904 | tf_op jit(solution)/shard_map/while/body/convert_element_type | solution.py:63
  193.0 5.3 %fusion.70 = (f32[4,256]{1,0:T(4,128)S(1)}, f32[4,256,1024]{1,2,0:T(8,128)S(1)}, f32[4,1024,256]{2,1,0:T(8,128)}) fusion(pred[256,1024]{0,1:T(8,128)(4,1)S(1)} %broadcast_compare_fusion.2, bf16[1024,4,64]{0,2,1:T(8,128)(2,1)S(1)} %bitcast.73, bf16[256,4,64]{0,2,1:T(8,128)(2,1)S(1)} %get-tuple-element.163), kind=kOutput, calls=%fused_computation.27.clone.1 | convolution fusion | flops 144702464 | bytes 9310208 | tf_op jit(solution)/shard_map/while/body/qhe,khe->hqk/dot_general | solution.py:57
  198.3 10.1 %fusion.71 = f32[4,256,8,128]{1,2,3,0:T(8,128)S(1)} fusion(f32[4,256,8,128]{1,3,2,0:T(8,128)S(1)} %bitcast.71), kind=kOutput, calls=%fused_computation.18.clone.1 | output fusion | flops 133169152 | bytes 8388608 | tf_op jit(solution)/shard_map/reduce-window
  208.4 2.0 copy-done.1
  210.5 2.6 broadcast_add_fusion.2
  215.3 6.6 %fusion.72 = bf16[4,256,1024]{1,2,0:T(8,128)(2,1)S(1)} fusion(f32[4,256,8,128]{1,3,2,0:T(8,128)S(1)} %copy.35, f32[4,1024,256]{2,1,0:T(8,128)S(1)} %copy-done.2, pred[256,1024]{0,1:T(8,128)(4,1)S(1)} %broadcast_compare_fusion.2), kind=kLoop, calls=%fused_computation.9.clone.1 | loop fusion | flops 22020096 | bytes 10747904 | tf_op jit(solution)/shard_map/while/body/convert_element_type | solution.py:63
  224.0 5.3 %fusion.70 = (f32[4,256]{1,0:T(4,128)S(1)}, f32[4,256,1024]{1,2,0:T(8,128)S(1)}, f32[4,1024,256]{2,1,0:T(8,128)}) fusion(pred[256,1024]{0,1:T(8,128)(4,1)S(1)} %broadcast_compare_fusion.2, bf16[1024,4,64]{0,2,1:T(8,128)(2,1)S(1)} %bitcast.73, bf16[256,4,64]{0,2,1:T(8,128)(2,1)S(1)} %get-tuple-element.163), kind=kOutput, calls=%fused_computation.27.clone.1 | convolution fusion | flops 144702464 | bytes 9310208 | tf_op jit(solution)/shard_map/while/body/qhe,khe->hqk/dot_general | solution.py:57
  229.3 10.1 %fusion.71 = f32[4,256,8,128]{1,2,3,0:T(8,128)S(1)} fusion(f32[4,256,8,128]{1,3,2,0:T(8,128)S(1)} %bitcast.71), kind=kOutput, calls=%fused_computation.18.clone.1 | output fusion | flops 133169152 | bytes 8388608 | tf_op jit(solution)/shard_map/reduce-window
  239.4 2.0 copy-done.1
  241.5 2.6 broadcast_add_fusion.2
  246.3 6.6 %fusion.72 = bf16[4,256,1024]{1,2,0:T(8,128)(2,1)S(1)} fusion(f32[4,256,8,128]{1,3,2,0:T(8,128)S(1)} %copy.35, f32[4,1024,256]{2,1,0:T(8,128)S(1)} %copy-done.2, pred[256,1024]{0,1:T(8,128)(4,1)S(1)} %broadcast_compare_fusion.2), kind=kLoop, calls=%fused_computation.9.clone.1 | loop fusion | flops 22020096 | bytes 10747904 | tf_op jit(solution)/shard_map/while/body/convert_element_type | solution.py:63
  255.0 5.3 %fusion.70 = (f32[4,256]{1,0:T(4,128)S(1)}, f32[4,256,1024]{1,2,0:T(8,128)S(1)}, f32[4,1024,256]{2,1,0:T(8,128)}) fusion(pred[256,1024]{0,1:T(8,128)(4,1)S(1)} %broadcast_compare_fusion.2, bf16[1024,4,64]{0,2,1:T(8,128)(2,1)S(1)} %bitcast.73, bf16[256,4,64]{0,2,1:T(8,128)(2,1)S(1)} %get-tuple-element.163), kind=kOutput, calls=%fused_computation.27.clone.1 | convolution fusion | flops 144702464 | bytes 9310208 | tf_op jit(solution)/shard_map/while/body/qhe,khe->hqk/dot_general | solution.py:57
  260.3 10.1 %fusion.71 = f32[4,256,8,128]{1,2,3,0:T(8,128)S(1)} fusion(f32[4,256,8,128]{1,3,2,0:T(8,128)S(1)} %bitcast.71), kind=kOutput, calls=%fused_computation.18.clone.1 | output fusion | flops 133169152 | bytes 8388608 | tf_op jit(solution)/shard_map/reduce-window
  270.4 2.0 copy-done.1
  272.5 2.6 broadcast_add_fusion.2
  277.3 6.6 %fusion.72 = bf16[4,256,1024]{1,2,0:T(8,128)(2,1)S(1)} fusion(f32[4,256,8,128]{1,3,2,0:T(8,128)S(1)} %copy.35, f32[4,1024,256]{2,1,0:T(8,128)S(1)} %copy-done.2, pred[256,1024]{0,1:T(8,128)(4,1)S(1)} %broadcast_compare_fusion.2), kind=kLoop, calls=%fused_computation.9.clone.1 | loop fusion | flops 22020096 | bytes 10747904 | tf_op jit(solution)/shard_map/while/body/convert_element_type | solution.py:63
  286.0 5.3 %fusion.70 = (f32[4,256]{1,0:T(4,128)S(1)}, f32[4,256,1024]{1,2,0:T(8,128)S(1)}, f32[4,1024,256]{2,1,0:T(8,128)}) fusion(pred[256,1024]{0,1:T(8,128)(4,1)S(1)} %broadcast_compare_fusion.2, bf16[1024,4,64]{0,2,1:T(8,128)(2,1)S(1)} %bitcast.73, bf16[256,4,64]{0,2,1:T(8,128)(2,1)S(1)} %get-tuple-element.163), kind=kOutput, calls=%fused_computation.27.clone.1 | convolution fusion | flops 144702464 | bytes 9310208 | tf_op jit(solution)/shard_map/while/body/qhe,khe->hqk/dot_general | solution.py:57
  291.3 10.1 %fusion.71 = f32[4,256,8,128]{1,2,3,0:T(8,128)S(1)} fusion(f32[4,256,8,128]{1,3,2,0:T(8,128)S(1)} %bitcast.71), kind=kOutput, calls=%fused_computation.18.clone.1 | output fusion | flops 133169152 | bytes 8388608 | tf_op jit(solution)/shard_map/reduce-window
  301.4 2.0 copy-done.1
  303.5 2.6 broadcast_add_fusion.2
  308.3 6.6 %fusion.72 = bf16[4,256,1024]{1,2,0:T(8,128)(2,1)S(1)} fusion(f32[4,256,8,128]{1,3,2,0:T(8,128)S(1)} %copy.35, f32[4,1024,256]{2,1,0:T(8,128)S(1)} %copy-done.2, pred[256,1024]{0,1:T(8,128)(4,1)S(1)} %broadcast_compare_fusion.2), kind=kLoop, calls=%fused_computation.9.clone.1 | loop fusion | flops 22020096 | bytes 10747904 | tf_op jit(solution)/shard_map/while/body/convert_element_type | solution.py:63
  317.0 5.3 %fusion.70 = (f32[4,256]{1,0:T(4,128)S(1)}, f32[4,256,1024]{1,2,0:T(8,128)S(1)}, f32[4,1024,256]{2,1,0:T(8,128)}) fusion(pred[256,1024]{0,1:T(8,128)(4,1)S(1)} %broadcast_compare_fusion.2, bf16[1024,4,64]{0,2,1:T(8,128)(2,1)S(1)} %bitcast.73, bf16[256,4,64]{0,2,1:T(8,128)(2,1)S(1)} %get-tuple-element.163), kind=kOutput, calls=%fused_computation.27.clone.1 | convolution fusion | flops 144702464 | bytes 9310208 | tf_op jit(solution)/shard_map/while/body/qhe,khe->hqk/dot_general | solution.py:57
  322.3 10.1 %fusion.71 = f32[4,256,8,128]{1,2,3,0:T(8,128)S(1)} fusion(f32[4,256,8,128]{1,3,2,0:T(8,128)S(1)} %bitcast.71), kind=kOutput, calls=%fused_computation.18.clone.1 | output fusion | flops 133169152 | bytes 8388608 | tf_op jit(solution)/shard_map/reduce-window
  334.5 2.6 broadcast_add_fusion.2
  339.3 6.6 %fusion.72 = bf16[4,256,1024]{1,2,0:T(8,128)(2,1)S(1)} fusion(f32[4,256,8,128]{1,3,2,0:T(8,128)S(1)} %copy.35, f32[4,1024,256]{2,1,0:T(8,128)S(1)} %copy-done.2, pred[256,1024]{0,1:T(8,128)(4,1)S(1)} %broadcast_compare_fusion.2), kind=kLoop, calls=%fused_computation.9.clone.1 | loop fusion | flops 22020096 | bytes 10747904 | tf_op jit(solution)/shard_map/while/body/convert_element_type | solution.py:63
  347.3 30.9 %all_to_all.15 = f32[4,64,2048]{2,1,0:T(8,128)S(1)} all-to-all(f32[4,64,2048]{2,1,0:T(8,128)S(1)} %fusion.26), channel_id=1, replica_groups=mesh['grp'=2,'sp'=32,'tp'=4] {'tp'}, dimensions={0} | all-to-all | bytes 4194304 | tf_op jit(solution)/shard_map/all_to_all | solution.py:29
  381.7 3.6 all-to-all-start.1
  385.3 14.5 %all-to-all-done.1 = bf16[4,64,2048]{2,1,0:T(8,128)(2,1)S(1)} async-done(((bf16[4,64,2048]{2,1,0:T(8,128)(2,1)}), bf16[4,64,2048]{2,1,0:T(8,128)(2,1)S(1)}, u32[]{:S(2)}, u32[]{:S(2)}) %all-to-all-start.1) | async-done | bytes 1048608 | tf_op jit(solution)/shard_map/all_to_all | solution.py:41
  399.9 3.0 fusion.20
  406.6 2.9 collective-permute-done
  409.8 3.3 fusion.38
  413.1 28.4 %all_to_all.16 = f32[4,64,2048]{2,1,0:T(8,128)S(1)} all-to-all(f32[4,64,2048]{2,1,0:T(8,128)S(1)} %bitcast.74), channel_id=1, replica_groups=mesh['grp'=2,'sp'=32,'tp'=4] {'tp'}, dimensions={0} | all-to-all | bytes 4194304 | tf_op jit(solution)/shard_map/all_to_all | solution.py:29
  (149 shorter events, 53.6 us)
Async XLA Ops:
  6.5 340.3 %copy-start = (bf16[256,2048]{1,0:T(8,128)(2,1)S(1)}, bf16[256,2048]{1,0:T(8,128)(2,1)}, u32[]{:S(2)}) copy-start(bf16[256,2048]{1,0:T(8,128)(2,1)} %param.17) | copy-start | bytes 3145732
  6.6 91.7 %all-gather.4.cloned.1.call-start = ((), (), s32[]{:S(2)}) async-start(), calls=%async_computation.3 | async-start | bytes 8650752 | tf_op jit(solution)/shard_map/all_gather | solution.py:109
  9.4 375.9 %all-gather.6.cloned.1.call-start = ((), (), s32[]{:S(2)}) async-start(), calls=%async_computation.4 | async-start | bytes 6488064 | tf_op jit(solution)/shard_map/all_gather | solution.py:18
  11.2 398.6 %all-gather.8.cloned.1.call-start = ((), (), s32[]{:S(2)}) async-start(), calls=%async_computation.5 | async-start | bytes 3244032 | tf_op jit(solution)/shard_map/all_gather | solution.py:107
  115.2 2.0 copy-start.1
  119.9 2.3 copy-start.2
  146.3 2.0 copy-start.1
  151.0 2.3 copy-start.2
  177.4 2.0 copy-start.1
  182.1 2.2 copy-start.2
  208.4 2.0 copy-start.1
  213.1 2.2 copy-start.2
  239.4 2.0 copy-start.1
  244.1 2.2 copy-start.2
  270.4 2.0 copy-start.1
  275.1 2.2 copy-start.2
  301.4 2.0 copy-start.1
  306.1 2.2 copy-start.2
  332.4 2.0 copy-start.1
  337.1 2.2 copy-start.2
  347.3 31.9 %copy-start.3 = (bf16[64,2048]{1,0:T(8,128)(2,1)S(1)}, bf16[64,2048]{1,0:T(8,128)(2,1)}, u32[]{:S(2)}) copy-start(bf16[64,2048]{1,0:T(8,128)(2,1)} %param.16) | copy-start | bytes 786436
  347.3 33.1 %copy-start.4 = (f32[2048]{0:T(1024)S(1)}, f32[2048]{0:T(1024)}, u32[]{:S(2)}) copy-start(f32[2048]{0:T(1024)} %param.22) | copy-start | bytes 24580
  381.7 18.2 %all-to-all-start.1 = ((bf16[4,64,2048]{2,1,0:T(8,128)(2,1)}), bf16[4,64,2048]{2,1,0:T(8,128)(2,1)S(1)}, u32[]{:S(2)}, u32[]{:S(2)}) async-start(bf16[4,64,2048]{2,1,0:T(8,128)(2,1)} %broadcast_in_dim.30), calls=%async_computation.1 | async-start | bytes 2097152 | tf_op jit(solution)/shard_map/all_to_all | solution.py:41
  399.9 3.7 copy-start.7
  402.9 3.7 copy-start.5
  402.9 3.7 copy-start.6
  404.6 5.0 %collective-permute-start = (bf16[2,1536]{1,0:T(2,128)(2,1)S(1)}, bf16[2,1536]{1,0:T(2,128)(2,1)S(1)}, u32[]{:S(2)}, u32[]{:S(2)}) collective-permute-start(bf16[2,1536]{1,0:T(2,128)(2,1)S(1)} %pad_maximum_fusion.2), channel_id=1, source_target_pairs={{0,4},{4,8},{8,12},{12,16},{16,20},{20,24},{24,28},{28,32},{32,36}... | collective-permute-start | bytes 18440 | tf_op jit(solution)/shard_map/ppermute | solution.py:53
Sparse Core Ops, SparseCore 0:
  9.6 88.6 all-gather.3
  100.1 70.6 all-gather.5
  172.6 67.8 all-gather.7
where the time goes:
time: 452 us; the launch traced here: 451 us
  other arithmetic  164 us (36%)
  waiting for transfers between devices  104 us (23%)
  blocking collectives  59.3 us (13%)
  matrix products  54.2 us (12%)
  local copies, waits for them, and re-layouts  49.3 us (11%)
  between operations  13.4 us (3%)
  starting transfers between devices  5.69 us (1%)
    all_gather x1, waiting for transfers between devices, body(): gathered = lax.all_gather(paired, 'sp', axis=0, tiled=True)  85.2 us
    another operation x16, other arithmetic  81.1 us
    all_to_all x2, blocking collectives, summed_on_arrival(): lax.all_to_all(pieces, axis, split_axis=0, concat_axis=0, tiled=True)  59.3 us
    convert_element_type x8, other arithmetic, block_terms(): jnp.where(causal, jnp.exp(jax.nn.log_sigmoid(scores) + suffix), 0.0)  52.8 us
    dot_general x8, matrix products, block_terms(): jnp.einsum('qhe,khe->hqk', query_rows, key_rows, preferred_element_type=j...  42.3 us
    while x32, local copies, waits for them, and re-layouts  23.5 us
    another operation x8, other arithmetic, block_terms(): suffix = lax.cumsum(stay_log, axis=2, reverse=True) - stay_log  21 us
    all_to_all x1, waiting for transfers between devices, from_everyone(): lax.all_to_all(jnp.broadcast_to(shard[None], (peers, *shard.shape)), axis...  14.5 us
  transfers between devices with their start and end apart: 5, of which 3 were waited for; matrix products, arithmetic and copies ran while one was open for 52% of the time, Pallas kernels for 0%

commit v1 on v0

v1 whole, which is shorter than its diff:
```python
import functools
import math

import jax
import jax.numpy as jnp
from jax import lax
from jax.experimental import pallas as pl
from jax.experimental.pallas import tpu as pltpu
from jax.sharding import PartitionSpec as P

HEAD = 64
LANES = 128
EPS = 1e-06
GROUPS = 4
HALO = 16
MESH = pl.DeviceIdType.MESH
F32 = jnp.float32
BF16 = jnp.bfloat16
LOG2E = math.log2(math.e)


def kernel(
    dims,
    q_ref, k_ref, v_ref, resid_ref, wo_ref, gw_ref, vw_ref, cg_ref, cv_ref, gain_ref, dw_ref,
    out_ref,
    pack, s1, s2, kv, qx, tri, acc, later, mo, m2, wo, wf, dpart, state, ext, gated, rsb, pf, rsr,
    s1_s, s1_r, s2_s, s2_r, s3_s, s3_r, sp_s, sp_r, cw_s, cw_r, cc_s, cc_r, wp_s, wp_r,
    wo_l, wo_s, wo_r, wop_s, wop_r, m2_s, m2_r, nx_s, nx_r, ha_s, ha_r, rs_s, rs_r, dp_s, dp_r,
):
    nx, nz, heads, tok, piece, width, ff, slab = dims
    half = piece // 2
    down_rows = ff // 2
    blocks = down_rows // slab
    strips = nz // GROUPS
    rows_group = strips * piece
    sp = lax.axis_index("sp")
    x = lax.axis_index("tp")
    z = lax.div(sp, 2)
    c = lax.rem(sp, 2)
    partner = z * 2 + 1 - c
    low = lambda rows: lax.broadcasted_iota(jnp.int32, (rows, LANES), 1) < HEAD
    swap = lambda a: pltpu.roll(a, HEAD, 1)

    def xat(d):
        return lax.rem(x + d + nx, nx)

    def zat(d):
        return lax.rem(z + d + nz, nz)

    def remote(src, dst, send, recv, **where):
        return pltpu.make_async_remote_copy(
            src_ref=src, dst_ref=dst, send_sem=send, recv_sem=recv, device_id=where,
            device_id_type=MESH,
        )

    def slab_rows(zz, cc):
        return pl.ds(pl.multiple_of((zz * 2 + cc) * slab, slab), slab)

    for xp in range(nx):
        at = xp * piece
        for p in range(heads // 2):
            cols = slice(p * LANES, (p + 1) * LANES)
            kk = k_ref[at : at + piece, cols].astype(F32)
            vv = v_ref[at : at + piece, cols].astype(F32)
            qq = q_ref[at : at + piece, cols].astype(F32)
            qr = swap(qq)
            keep = low(piece)
            pack[xp, 2 * p, 0:piece] = jnp.where(keep, kk, swap(vv)).astype(BF16)
            pack[xp, 2 * p + 1, 0:piece] = jnp.where(keep, swap(kk), vv).astype(BF16)
            keep = low(half)
            pack[xp, 2 * p, piece:] = jnp.where(keep, qq[:half], qr[half:]).astype(BF16)
            pack[xp, 2 * p + 1, piece:] = jnp.where(keep, qr[:half], qq[half:]).astype(BF16)
    s1[x] = pack[x]
    wf[slab_rows(z, c), 0:ff] = gw_ref[...]
    wf[slab_rows(z, c), ff : 2 * ff] = vw_ref[...]

    own_wo = pltpu.make_async_copy(wo_ref, wo.at[x], wo_l)
    own_wo.start()

    barrier = pltpu.get_barrier_semaphore()
    last_x = x == nx - 1
    before = lax.rem(sp + 2 * nz - 1, 2 * nz)
    after = lax.rem(sp + 1, 2 * nz)

    def greet(**where):
        pl.semaphore_signal(barrier, inc=1, device_id=where, device_id_type=MESH)

    for d in range(1, nx):
        greet(tp=xat(d))
    for d in range(1, nz):
        greet(sp=zat(d) * 2 + c)
    greet(sp=partner)
    greet(sp=before, tp=nx - 1)

    @pl.when(last_x)
    def _():
        for xp in range(nx):
            greet(sp=after, tp=xp)

    pl.semaphore_wait(barrier, nx - 1 + nz - 1 + 2 + jnp.where(last_x, nx, 0))

    ends = []
    for d in range(1, nx):
        copy = remote(pack.at[xat(d)], s1.at[x], s1_s.at[d - 1], s1_r.at[d - 1], tp=xat(d))
        copy.start()
        ends.append(copy)
    down_part = remote(
        dw_ref.at[pl.ds(pl.multiple_of((1 - c) * down_rows, slab), down_rows)], dpart, dp_s, dp_r,
        sp=partner,
    )
    down_part.start()
    ends.append(down_part)
    share = wo_ref.shape[0] // 2
    own_half = pl.ds(pl.multiple_of(c * share, share), share)
    for d in range(1, nx):
        copy = remote(
            wo_ref.at[own_half], wo.at[x, own_half], wo_s.at[d - 1], wo_r.at[d - 1], tp=xat(d)
        )
        copy.start()
        ends.append(copy)

    down_part.wait_recv()
    mine = dw_ref[pl.ds(pl.multiple_of(c * down_rows, slab), down_rows), :].astype(F32)
    other = dpart[...].astype(F32)
    first = c == 0
    row = lax.broadcasted_iota(jnp.int32, (HEAD, LANES), 0)
    col = lax.broadcasted_iota(jnp.int32, (HEAD, LANES), 1)
    place_low = (row == col).astype(BF16)
    place_high = (row + HEAD == col).astype(BF16)
    both = jnp.dot(
        jnp.where(first, mine, other).astype(BF16), place_low, preferred_element_type=F32
    ) + jnp.dot(jnp.where(first, other, mine).astype(BF16), place_high, preferred_element_type=F32)
    both = both.astype(BF16)
    for j in range(blocks):
        wf[slab_rows(z, c), 2 * ff + j * LANES : 2 * ff + (j + 1) * LANES] = both[
            j * slab : (j + 1) * slab
        ]
    up_hops = nz // 2
    down_hops = nz - 1 - up_hops

    def pass_slab(origin, step):
        rows = wf.at[slab_rows(origin, c)]
        return rows

    def send_up(step):
        rows = pass_slab(zat(-step), step)
        copy = remote(rows, rows, cw_s.at[step], cw_r.at[step], sp=zat(1) * 2 + c)
        copy.start()
        ends.append(copy)

    def send_down(step):
        rows = pass_slab(zat(step), step)
        copy = remote(rows, rows, cc_s.at[step], cc_r.at[step], sp=zat(-1) * 2 + c)
        copy.start()
        ends.append(copy)

    def send_across(origin, index):
        rows = pass_slab(origin, index)
        copy = remote(rows, rows, wp_s.at[index], wp_r.at[index], sp=partner)
        copy.start()
        ends.append(copy)

    send_up(0)
    send_down(0)
    send_across(z, 0)

    def serve(step):
        if step <= up_hops:
            rows = pass_slab(zat(-step), step)
            remote(rows, rows, cw_s.at[step - 1], cw_r.at[step - 1], sp=zat(1) * 2 + c).wait_recv()
            if step < up_hops:
                send_up(step)
            send_across(zat(-step), step)
        if step <= down_hops:
            rows = pass_slab(zat(step), step)
            remote(rows, rows, cc_s.at[step - 1], cc_r.at[step - 1], sp=zat(-1) * 2 + c).wait_recv()
            if step < down_hops:
                send_down(step)
            send_across(zat(step), nz - step)

    for d in range(1, nx):
        remote(
            pack.at[x], s1.at[xat(-d)], s1_s.at[d - 1], s1_r.at[d - 1], tp=xat(d)
        ).wait_recv()
    s2[z] = s1[lax.div(z, heads), lax.rem(z, heads)]
    order = sorted(range(1, nz), key=lambda d: (min(d, nz - d), d))
    for d in order:
        h = zat(d)
        copy = remote(
            s1.at[lax.div(h, heads), lax.rem(h, heads)], s2.at[z], s2_s.at[d - 1], s2_r.at[d - 1],
            sp=h * 2 + c,
        )
        copy.start()
        ends.append(copy)

    r = lax.broadcasted_iota(jnp.int32, (tok, tok), 0)
    s = lax.broadcasted_iota(jnp.int32, (tok, tok), 1)
    tri[...] = (r > s).astype(BF16)
    acc[...] = jnp.zeros_like(acc)
    later[...] = jnp.zeros_like(later)
    for d in [0] + order:
        zs = zat(-d)
        if d:
            remote(
                s2.at[z], s2.at[zs], s2_s.at[d - 1], s2_r.at[d - 1], sp=zat(d) * 2 + c
            ).wait_recv()
        kv[zs, c, x] = s2[zs, 0:piece]
        for e in range(1, nx):
            remote(
                s2.at[zs, 0:piece], kv.at[zs, c, x], s3_s.at[e - 1], s3_r.at[e - 1], tp=xat(e)
            ).start()
        packed = s2[zs, piece:].astype(F32)
        keep = low(half)
        at = pl.multiple_of(zs * piece, piece)
        qx[pl.ds(at, half)] = jnp.where(keep, packed, 0.0).astype(BF16)
        qx[pl.ds(pl.multiple_of(at + half, half), half)] = jnp.where(
            keep, swap(packed), 0.0
        ).astype(BF16)
    across = remote(
        s2.at[:, 0:piece], kv.at[:, c, x], sp_s.at[0], sp_r.at[0], sp=partner
    )
    across.start()
    ends.append(across)
    serve(1)
    for e in (1, nx - 1) + tuple(range(2, nx - 1)) if nx > 2 else (1,):
        source = xat(-e)
        got = kv.at[:, c, source]
        remote(
            s2.at[:, 0:piece], got, s3_s.at[e - 1], s3_r.at[e - 1], tp=xat(e)
        ).wait_recv()
        across = remote(got, got, sp_s.at[e], sp_r.at[e], sp=partner)
        across.start()
        ends.append(across)
    for e in range(nx):
        there = kv.at[:, 1 - c, xat(-e)]
        remote(there, there, sp_s.at[e], sp_r.at[e], sp=partner).wait_recv()
    serve(2)

    scale = LOG2E / math.sqrt(HEAD)

    def tile_step(j, g, masked):
        rows = slice(g * rows_group, (g + 1) * rows_group)
        tile = kv[lax.div(j, 2), lax.rem(j, 2)].reshape(tok, LANES)
        score = lax.dot_general(
            qx[rows], tile, (((1,), (1,)), ((), ())), preferred_element_type=F32
        ) * scale
        neg = jnp.minimum(score, 0.0)
        pos = jnp.maximum(score, 0.0)
        soft = jnp.log(1.0 + jnp.exp2(neg - pos)) * LOG2E
        stay = pos + soft
        if masked:
            row = lax.broadcasted_iota(jnp.int32, (rows_group, 1), 0)
            strip = lax.div(row, piece)
            place = (g * strips + strip) * (2 * tok) + c * tok + x * piece + (row - strip * piece)
            seen = lax.broadcasted_iota(jnp.int32, (rows_group, tok), 1) < place - j * tok
            stay = jnp.where(seen, stay, 0.0)
        stay = stay.astype(BF16)
        suffix = jnp.dot(stay, tri[...], preferred_element_type=F32)
        behind = later[rows]
        whole = jnp.concatenate([behind] * (tok // LANES), axis=1)
        weight = jnp.exp2(neg - soft - suffix - whole)
        if masked:
            weight = jnp.where(seen, weight, 0.0)
        acc[rows] += jnp.dot(weight.astype(BF16), tile, preferred_element_type=F32)
        total = suffix[:, 0:1] + stay[:, 0:1].astype(F32)
        later[rows] = behind + jnp.broadcast_to(total, (rows_group, LANES))

    for low_group in reversed(range(GROUPS)):
        tiles = 2 * strips

        def step(i, carry, low_group=low_group, tiles=tiles):
            j = tiles * (low_group + 1) - 1 - i
            for g in range(low_group, GROUPS):
                tile_step(j, g, g == low_group)
            return carry

        lax.fori_loop(0, tiles, step, 0)
        if low_group:
            serve(3 + GROUPS - 1 - low_group)

    for zs in range(nz):
        rows = acc[zs * piece : (zs + 1) * piece]
        mo[zs] = jnp.where(low(half), swap(rows[:half]), rows[half:]).astype(BF16)
    m2[z] = mo[z]
    for d in order:
        h = zat(d)
        copy = remote(mo.at[h], m2.at[z], m2_s.at[d - 1], m2_r.at[d - 1], sp=h * 2 + c)
        copy.start()
        ends.append(copy)

    own_wo.wait()
    for d in range(1, nx):
        got = wo.at[xat(-d), own_half]
        remote(wo_ref.at[own_half], got, wo_s.at[d - 1], wo_r.at[d - 1], tp=xat(d)).wait_recv()
        copy = remote(got, got, wop_s.at[d - 1], wop_r.at[d - 1], sp=partner)
        copy.start()
        ends.append(copy)
    other_half = pl.ds(pl.multiple_of((1 - c) * share, share), share)
    for d in range(1, nx):
        there = wo.at[xat(-d), other_half]
        remote(there, there, wop_s.at[d - 1], wop_r.at[d - 1], sp=partner).wait_recv()
    for d in order:
        zs = zat(-d)
        remote(mo.at[z], m2.at[zs], m2_s.at[d - 1], m2_r.at[d - 1], sp=zat(d) * 2 + c).wait_recv()
    serve(6)

    top, bottom = [], []
    keep = low(half)
    for p in range(nz // 2):
        a, b = m2[2 * p].astype(F32), m2[2 * p + 1].astype(F32)
        top.append(jnp.where(keep, a, swap(b)).astype(BF16))
        bottom.append(jnp.where(keep, swap(a), b).astype(BF16))
    mixed = jnp.concatenate(
        [jnp.concatenate(top, axis=1), jnp.concatenate(bottom, axis=1)], axis=0
    )
    chunk = min(512, width)
    square = jnp.zeros((piece, 1), F32)
    for n in range(width // chunk):
        cols = slice(n * chunk, (n + 1) * chunk)
        weight = wo[:, :, cols].reshape(nx * wo.shape[1], chunk)
        added = resid_ref[:, cols].astype(F32) + jnp.dot(
            mixed, weight, preferred_element_type=F32
        )
        added = added.astype(BF16)
        state[:, cols] = added
        added = added.astype(F32)
        square += jnp.sum(added * added, axis=1, keepdims=True)
    factor = lax.rsqrt(square / width + EPS)
    mine_rows = pl.ds(pl.multiple_of(HALO + x * piece, HALO), piece)
    ext[mine_rows] = (state[...].astype(F32) * factor * gain_ref[...]).astype(BF16)

    for d in range(1, nx):
        rows = ext.at[mine_rows]
        copy = remote(rows, rows, nx_s.at[d - 1], nx_r.at[d - 1], tp=xat(d))
        copy.start()
        ends.append(copy)

    rim = ext.at[nx * piece : nx * piece + HALO]
    rims = [
        remote(rim, ext.at[0:HALO], ha_s.at[xp], ha_r, sp=after, tp=xp) for xp in range(nx)
    ]

    @pl.when(last_x)
    def _():
        for copy in rims:
            copy.start()

    serve(7)
    serve(8)
    for d in range(1, nx):
        rows = ext.at[pl.ds(pl.multiple_of(HALO + xat(-d) * piece, HALO), piece)]
        remote(rows, rows, nx_s.at[d - 1], nx_r.at[d - 1], tp=xat(d)).wait_recv()
    rims[0].wait_recv()

    @pl.when(sp == 0)
    def _():
        ext[0:HALO] = jnp.zeros((HALO, width), BF16)

    for index in range(nz):
        there = wf.at[slab_rows(zat(-index), 1 - c)]
        remote(there, there, wp_s.at[index], wp_r.at[index], sp=partner).wait_recv()

    chunk = min(256, ff)

    def conv(pre, taps, cols):
        pre = pre.astype(BF16).astype(F32)
        count = taps.shape[0]
        total = taps[0:1, cols] * pre[HALO - count + 1 : HALO - count + 1 + tok]
        for i in range(1, count):
            at = HALO - count + 1 + i
            total = total + taps[i : i + 1, cols] * pre[at : at + tok]
        return total

    for n in range(ff // chunk):
        cols = slice(n * chunk, (n + 1) * chunk)
        gate = jnp.dot(ext[...], wf[:, cols], preferred_element_type=F32)
        value = jnp.dot(
            ext[...], wf[:, ff + n * chunk : ff + (n + 1) * chunk], preferred_element_type=F32
        )
        gate = conv(gate, cg_ref, cols)
        value = conv(value, cv_ref, cols)
        gated[:, cols] = (gate / (1.0 + jnp.exp(-gate)) * value).astype(BF16)

    def rs_copy(d, cols):
        return remote(
            rsb.at[pl.ds(pl.multiple_of(xat(d) * piece, piece), piece), cols],
            rsr.at[d - 1, :, cols], rs_s.at[d - 1], rs_r.at[d - 1], tp=xat(d),
        )

    far_first = sorted(range(1, nx), key=lambda d: -min(d, nx - d))
    for n in range(nz // 2):
        sides = []
        for zz in (2 * n, 2 * n + 1):
            sides.append(
                jnp.concatenate(
                    [
                        wf[
                            (zz * 2 + cc) * slab : (zz * 2 + cc + 1) * slab,
                            2 * ff + j * LANES : 2 * ff + (j + 1) * LANES,
                        ]
                        for cc in range(2)
                        for j in range(blocks)
                    ],
                    axis=0,
                )
            )
        part = jnp.dot(
            gated[...], jnp.concatenate(sides, axis=1), preferred_element_type=F32
        )
        cols = slice(n * 2 * LANES, (n + 1) * 2 * LANES)
        pf[:, cols] = part
        rsb[:, cols] = part.astype(BF16)
        for d in far_first:
            rs_copy(d, cols).start()
    everything = slice(0, width)
    total = state[...].astype(F32) + pf[pl.ds(pl.multiple_of(x * piece, piece), piece)]
    for d in range(1, nx):
        rs_copy(d, everything).wait_recv()
        total = total + rsr[d - 1].astype(F32)
    out_ref[...] = total.astype(BF16)

    for copy in ends:
        copy.wait_send()
    for e in range(1, nx):
        remote(
            s2.at[:, 0:piece], kv.at[:, c, x], s3_s.at[e - 1], s3_r.at[e - 1], tp=xat(e)
        ).wait_send()
        rs_copy(e, everything).wait_send()

    @pl.when(last_x)
    def _():
        for copy in rims:
            copy.wait_send()


def body(*args):
    queries, keys, values, resid, out_weight, gate_weight = args[:6]
    nx, nz = lax.axis_size("tp"), lax.axis_size("sp") // 2
    tok, mix = queries.shape
    piece, width = resid.shape
    ff = gate_weight.shape[1]
    slab = gate_weight.shape[0]
    heads = mix // HEAD
    assert heads * nx == nz
    blocks = ff // 2 // slab
    dims = (nx, nz, heads, tok, piece, width, ff, slab)
    packed = piece + piece // 2
    vmem = pltpu.VMEM
    dma = pltpu.SemaphoreType.DMA
    scratch = [
        vmem((nx, heads, packed, LANES), BF16),
        vmem((nx, heads, packed, LANES), BF16),
        vmem((nz, packed, LANES), BF16),
        vmem((nz, 2, nx, piece, LANES), BF16),
        vmem((nz * piece, LANES), BF16),
        vmem((tok, tok), BF16),
        vmem((nz * piece, LANES), F32),
        vmem((nz * piece, LANES), F32),
        vmem((nz, piece // 2, LANES), BF16),
        vmem((nz, piece // 2, LANES), BF16),
        vmem((nx, out_weight.shape[0], width), BF16),
        vmem((2 * nz * slab, 2 * ff + blocks * LANES), BF16),
        vmem((ff // 2, HEAD), BF16),
        vmem((piece, width), BF16),
        vmem((HALO + tok, width), BF16),
        vmem((tok, ff), BF16),
        vmem((tok, width), BF16),
        vmem((tok, width), F32),
        vmem((nx - 1, piece, width), BF16),
    ]
    sems = [
        dma((nx - 1,)), dma((nx - 1,)),
        dma((nz - 1,)), dma((nz - 1,)),
        dma((nx - 1,)), dma((nx - 1,)),
        dma((nx,)), dma((nx,)),
        dma((nz // 2,)), dma((nz // 2,)),
        dma((nz - 1 - nz // 2,)), dma((nz - 1 - nz // 2,)),
        dma((nz,)), dma((nz,)),
        dma, dma((nx - 1,)), dma((nx - 1,)),
        dma((nx - 1,)), dma((nx - 1,)),
        dma((nz - 1,)), dma((nz - 1,)),
        dma((nx - 1,)), dma((nx - 1,)),
        dma((nx,)), dma,
        dma((nx - 1,)), dma((nx - 1,)),
        dma, dma,
    ]
    in_vmem = pl.BlockSpec(memory_space=pltpu.VMEM)
    specs = [in_vmem] * 11
    specs[4] = pl.BlockSpec(memory_space=pl.ANY)
    args = list(args)
    args[9] = args[9].reshape(1, width)
    return pl.pallas_call(
        functools.partial(kernel, dims),
        out_shape=jax.ShapeDtypeStruct((piece, width), BF16),
        in_specs=specs,
        out_specs=in_vmem,
        scratch_shapes=scratch + sems,
        compiler_params=pltpu.CompilerParams(
            collective_id=0, has_side_effects=True, vmem_limit_bytes=48 * 1024 * 1024
        ),
        name="layer",
    )(*args)


def solution(mesh):
    placed = (
        P(("grp", "sp"), "tp"),
        P(("grp", "sp"), "tp"),
        P(("grp", "sp"), "tp"),
        P(("grp", "sp", "tp"), None),
        P("tp", None),
        P("sp", "tp"),
        P("sp", "tp"),
        P(None, "tp"),
        P(None, "tp"),
        P(),
        P("tp", "sp"),
    )
    return jax.shard_map(
        body, mesh=mesh, in_specs=placed, out_specs=P(("grp", "sp", "tp"), None), check_vma=False
    )
```

time: 452 us -> 160 us (0.35)
  the two profiles are of different devices: /device:TPU:1824 before, /device:TPU:33 now
where the time goes in v1:
time: 160 us
  Pallas kernels  152 us (95%)
  local copies, waits for them, and re-layouts  7.53 us (5%)
    pallas_call x1, Pallas kernels, body(): pl.pallas_call(functools.partial(kernel, dims), out_shape=jax.ShapeDtypeS...  152 us
    unnamed x22, local copies, waits for them, and re-layouts  7.53 us

profile of v1, /device:TPU:33, one launch (start us, length us, event | category | flops | bytes accessed | tf_op | source)
XLA Modules:
  0.0 159.6 jit_solution(12901150227965910941)
XLA Ops:
  0.0 0.0 copy-start.1
  0.0 0.0 copy-start.7
  0.0 0.0 copy-start.8
  0.0 0.0 copy-start.9
  0.0 1.1 copy.12.dw_ref
  1.1 0.0 copy-done.1
  1.1 0.0 copy-done.7
  1.1 0.0 copy-done.8
  1.1 0.0 copy-done.9
  1.2 0.0 copy-start
  1.2 1.2 copy-done
  2.4 0.0 copy-start.2
  2.4 0.9 copy-done.2
  3.3 0.0 copy-start.3
  3.3 0.9 copy-done.3
  4.2 0.0 copy-start.4
  4.2 0.9 copy-done.4
  5.1 0.0 copy-start.5
  5.1 0.9 copy-done.5
  6.0 0.0 copy-start.6
  6.0 0.9 copy-done.6
  6.9 151.9 %layer.1 = bf16[64,2048]{1,0:T(8,128)(2,1)S(1)} custom-call(bf16[256,256]{1,0:T(8,128)(2,1)S(1)} %copy-done.2, bf16[256,256]{1,0:T(8,128)(2,1)S(1)} %copy-done.3, bf16[256,256]{1,0:T(8,128)(2,1)S(1)} %copy-done.4, bf16[64,2048]{1,0:T(8,128)(2,1)S(1)} %copy-done.1, bf16[256,2048]{1,0:T(8,128)(2,1)S(1)} %copy-done, bf16[64,768]{1,0:T(8,128)(2,1)S(1)} %copy-done.5, ...), custom_call_target="tpu_custom_call" | custom-call | tf_op jit(solution)/shard_map/layer/pallas_call | solution.py:492
  158.8 0.7 copy.14
Async XLA Ops:
  0.0 1.1 copy-start.1
  0.0 1.1 copy-start.7
  0.0 1.1 copy-start.8
  0.0 1.1 copy-start.9
  1.2 1.2 copy-start
  2.4 0.9 copy-start.2
  3.3 0.9 copy-start.3
  4.2 0.9 copy-start.4
  5.1 0.9 copy-start.5
  6.0 0.9 copy-start.6

commit v2 on v1

--- a/solution.py
+++ b/solution.py
@@ -21,10 +21,10 @@
 
 def kernel(
     dims,
-    q_ref, k_ref, v_ref, resid_ref, wo_ref, gw_ref, vw_ref, cg_ref, cv_ref, gain_ref, dw_ref,
+    q_hbm, k_hbm, v_hbm, resid_hbm, wo_ref, gw_ref, vw_ref, cg_ref, cv_ref, gain_ref, dw_ref,
     out_ref,
-    pack, s1, s2, kv, qx, tri, acc, later, mo, m2, wo, wf, dpart, state, ext, gated, rsb, pf, rsr,
-    s1_s, s1_r, s2_s, s2_r, s3_s, s3_r, sp_s, sp_r, cw_s, cw_r, cc_s, cc_r, wp_s, wp_r,
+    q_ref, k_ref, v_ref, resid_ref, dwn, place, pack, s1, s2, kv, qx, tri, acc, later, mo, m2, wo, wf, dpart, state, ext, gated, rsb, pf, rsr,
+    s1_s, s1_r, s2_s, s2_r, s3_s, s3_r, sp_s, sp_r, in_l, cw_s, cw_r, cc_s, cc_r, wp_s, wp_r,
     wo_l, wo_s, wo_r, wop_s, wop_r, m2_s, m2_r, nx_s, nx_r, ha_s, ha_r, rs_s, rs_r, dp_s, dp_r,
 ):
     nx, nz, heads, tok, piece, width, ff, slab = dims
@@ -56,6 +56,25 @@
     def slab_rows(zz, cc):
         return pl.ds(pl.multiple_of((zz * 2 + cc) * slab, slab), slab)
 
+    loads = []
+    for i, (src, dst) in enumerate(
+        (
+            (q_hbm, q_ref),
+            (k_hbm, k_ref),
+            (v_hbm, v_ref),
+            (dw_ref.at[:, pl.ds(pl.multiple_of(c * down_rows, LANES), down_rows)], dwn),
+            (gw_ref, wf.at[slab_rows(z, c), 0:ff]),
+            (vw_ref, wf.at[slab_rows(z, c), ff : 2 * ff]),
+            (resid_hbm, resid_ref),
+        )
+    ):
+        loads.append(pltpu.make_async_copy(src, dst, in_l.at[i]))
+        loads[-1].start()
+    own_wo = pltpu.make_async_copy(wo_ref, wo.at[x], wo_l)
+    own_wo.start()
+    for load in loads[:3]:
+        load.wait()
+
     for xp in range(nx):
         at = xp * piece
         for p in range(heads // 2):
@@ -71,11 +90,6 @@
             pack[xp, 2 * p, piece:] = jnp.where(keep, qq[:half], qr[half:]).astype(BF16)
             pack[xp, 2 * p + 1, piece:] = jnp.where(keep, qr[:half], qq[half:]).astype(BF16)
     s1[x] = pack[x]
-    wf[slab_rows(z, c), 0:ff] = gw_ref[...]
-    wf[slab_rows(z, c), ff : 2 * ff] = vw_ref[...]
-
-    own_wo = pltpu.make_async_copy(wo_ref, wo.at[x], wo_l)
-    own_wo.start()
 
     barrier = pltpu.get_barrier_semaphore()
     last_x = x == nx - 1
@@ -105,78 +119,89 @@
         copy.start()
         ends.append(copy)
     down_part = remote(
-        dw_ref.at[pl.ds(pl.multiple_of((1 - c) * down_rows, slab), down_rows)], dpart, dp_s, dp_r,
-        sp=partner,
+        dw_ref.at[:, pl.ds(pl.multiple_of((1 - c) * down_rows, LANES), down_rows)], dpart, dp_s,
+        dp_r, sp=partner,
     )
     down_part.start()
     ends.append(down_part)
     share = wo_ref.shape[0] // 2
     own_half = pl.ds(pl.multiple_of(c * share, share), share)
-    for d in range(1, nx):
-        copy = remote(
-            wo_ref.at[own_half], wo.at[x, own_half], wo_s.at[d - 1], wo_r.at[d - 1], tp=xat(d)
-        )
-        copy.start()
-        ends.append(copy)
+    wo_parts = nz
+    wo_cols = width // wo_parts
+
+    def send_wo(part):
+        cols = slice(part * wo_cols, (part + 1) * wo_cols)
+        for d in range(1, nx):
+            remote(
+                wo_ref.at[own_half, cols], wo.at[x, own_half, cols], wo_s.at[d - 1],
+                wo_r.at[d - 1], tp=xat(d),
+            ).start()
 
     down_part.wait_recv()
-    mine = dw_ref[pl.ds(pl.multiple_of(c * down_rows, slab), down_rows), :].astype(F32)
+    for load in loads[3:6]:
+        load.wait()
+    mine = dwn[...].astype(F32)
     other = dpart[...].astype(F32)
     first = c == 0
     row = lax.broadcasted_iota(jnp.int32, (HEAD, LANES), 0)
     col = lax.broadcasted_iota(jnp.int32, (HEAD, LANES), 1)
-    place_low = (row == col).astype(BF16)
-    place_high = (row + HEAD == col).astype(BF16)
-    both = jnp.dot(
-        jnp.where(first, mine, other).astype(BF16), place_low, preferred_element_type=F32
-    ) + jnp.dot(jnp.where(first, other, mine).astype(BF16), place_high, preferred_element_type=F32)
+    turn = (((0,), (0,)), ((), ()))
+    both = lax.dot_general(
+        jnp.where(first, mine, other).astype(BF16), (row == col).astype(BF16), turn,
+        preferred_element_type=F32,
+    ) + lax.dot_general(
+        jnp.where(first, other, mine).astype(BF16), (row + HEAD == col).astype(BF16), turn,
+        preferred_element_type=F32,
+    )
     both = both.astype(BF16)
     for j in range(blocks):
         wf[slab_rows(z, c), 2 * ff + j * LANES : 2 * ff + (j + 1) * LANES] = both[
             j * slab : (j + 1) * slab
         ]
-    up_hops = nz // 2
-    down_hops = nz - 1 - up_hops
-
-    def pass_slab(origin, step):
-        rows = wf.at[slab_rows(origin, c)]
-        return rows
-
-    def send_up(step):
-        rows = pass_slab(zat(-step), step)
-        copy = remote(rows, rows, cw_s.at[step], cw_r.at[step], sp=zat(1) * 2 + c)
+    hops = (nz // 2, nz - 1 - nz // 2)
+    lanes = (slice(0, 2 * ff), slice(2 * ff, 2 * ff + blocks * LANES))
+
+    def ring(way, kind, step):
+        origin = zat(-step) if way == 0 else zat(step)
+        part = wf.at[slab_rows(origin, c), lanes[kind]]
+        sends, recvs = ((cw_s, cw_r), (cc_s, cc_r))[way]
+        to = zat(1) if way == 0 else zat(-1)
+        return remote(part, part, sends.at[kind, step], recvs.at[kind, step], sp=to * 2 + c)
+
+    def come(way, kind, step):
+        origin = zat(-step) if way == 0 else zat(step)
+        part = wf.at[slab_rows(origin, c), lanes[kind]]
+        sends, recvs = ((cw_s, cw_r), (cc_s, cc_r))[way]
+        to = zat(1) if way == 0 else zat(-1)
+        return remote(
+            part, part, sends.at[kind, step - 1], recvs.at[kind, step - 1], sp=to * 2 + c
+        )
+
+    def begin(copy):
         copy.start()
         ends.append(copy)
 
-    def send_down(step):
-        rows = pass_slab(zat(step), step)
-        copy = remote(rows, rows, cc_s.at[step], cc_r.at[step], sp=zat(-1) * 2 + c)
-        copy.start()
-        ends.append(copy)
-
-    def send_across(origin, index):
-        rows = pass_slab(origin, index)
-        copy = remote(rows, rows, wp_s.at[index], wp_r.at[index], sp=partner)
-        copy.start()
-        ends.append(copy)
-
-    send_up(0)
-    send_down(0)
-    send_across(z, 0)
+    def send_across(origin, kind, index):
+        part = wf.at[slab_rows(origin, c), lanes[kind]]
+        begin(remote(part, part, wp_s.at[kind, index], wp_r.at[kind, index], sp=partner))
+
+    for kind in range(2):
+        for way in range(2):
+            begin(ring(way, kind, 0))
+    for kind in range(2):
+        send_across(z, kind, 0)
 
     def serve(step):
-        if step <= up_hops:
-            rows = pass_slab(zat(-step), step)
-            remote(rows, rows, cw_s.at[step - 1], cw_r.at[step - 1], sp=zat(1) * 2 + c).wait_recv()
-            if step < up_hops:
-                send_up(step)
-            send_across(zat(-step), step)
-        if step <= down_hops:
-            rows = pass_slab(zat(step), step)
-            remote(rows, rows, cc_s.at[step - 1], cc_r.at[step - 1], sp=zat(-1) * 2 + c).wait_recv()
-            if step < down_hops:
-                send_down(step)
-            send_across(zat(step), nz - step)
+        for kind in range(2):
+            at = step - kind
+            for way in range(2):
+                if 1 <= at <= hops[way]:
+                    come(way, kind, at).wait_recv()
+                    if at < hops[way]:
+                        begin(ring(way, kind, at))
+                    send_across(
+                        zat(-at) if way == 0 else zat(at), kind, at if way == 0 else nz - at
+                    )
 
     for d in range(1, nx):
         remote(
@@ -196,10 +221,15 @@
     r = lax.broadcasted_iota(jnp.int32, (tok, tok), 0)
     s = lax.broadcasted_iota(jnp.int32, (tok, tok), 1)
     tri[...] = (r > s).astype(BF16)
+    row = lax.broadcasted_iota(jnp.int32, (nz * piece, LANES), 0)
+    strip = lax.div(row, piece)
+    place[...] = strip * (2 * tok - piece) + row + c * tok + x * piece
     acc[...] = jnp.zeros_like(acc)
     later[...] = jnp.zeros_like(later)
-    for d in [0] + order:
+    for number, d in enumerate([0] + order):
         zs = zat(-d)
+        if number < wo_parts // 2:
+            send_wo(number)
         if d:
             remote(
                 s2.at[z], s2.at[zs], s2_s.at[d - 1], s2_r.at[d - 1], sp=zat(d) * 2 + c
@@ -221,6 +251,8 @@
     )
     across.start()
     ends.append(across)
+    for part in range(wo_parts // 2, wo_parts):
+        send_wo(part)
     serve(1)
     for e in (1, nx - 1) + tuple(range(2, nx - 1)) if nx > 2 else (1,):
         source = xat(-e)
@@ -238,45 +270,63 @@
 
     scale = LOG2E / math.sqrt(HEAD)
 
-    def tile_step(j, g, masked):
-        rows = slice(g * rows_group, (g + 1) * rows_group)
+    def group_rows(g):
+        return slice(g * rows_group, (g + 1) * rows_group)
+
+    def chances(j, g, masked):
         tile = kv[lax.div(j, 2), lax.rem(j, 2)].reshape(tok, LANES)
         score = lax.dot_general(
-            qx[rows], tile, (((1,), (1,)), ((), ())), preferred_element_type=F32
+            qx[group_rows(g)], tile, (((1,), (1,)), ((), ())), preferred_element_type=F32
         ) * scale
         neg = jnp.minimum(score, 0.0)
         pos = jnp.maximum(score, 0.0)
-        soft = jnp.log(1.0 + jnp.exp2(neg - pos)) * LOG2E
+        soft = jnp.log2(1.0 + jnp.exp2(neg - pos))
         stay = pos + soft
+        seen = None
         if masked:
-            row = lax.broadcasted_iota(jnp.int32, (rows_group, 1), 0)
-            strip = lax.div(row, piece)
-            place = (g * strips + strip) * (2 * tok) + c * tok + x * piece + (row - strip * piece)
-            seen = lax.broadcasted_iota(jnp.int32, (rows_group, tok), 1) < place - j * tok
+            where = jnp.concatenate([place[group_rows(g)]] * (tok // LANES), axis=1)
+            seen = lax.broadcasted_iota(jnp.int32, (rows_group, tok), 1) < where - j * tok
             stay = jnp.where(seen, stay, 0.0)
-        stay = stay.astype(BF16)
+        return tile, neg - soft, stay.astype(BF16), seen
+
+    def weights(tile, go, stay, seen):
         suffix = jnp.dot(stay, tri[...], preferred_element_type=F32)
+        weight = jnp.exp2(go - suffix)
+        if seen is not None:
+            weight = jnp.where(seen, weight, 0.0)
+        return tile, weight.astype(BF16), suffix[:, 0:1] + stay[:, 0:1].astype(F32)
+
+    def gather(g, tile, weight, total):
+        rows = group_rows(g)
         behind = later[rows]
-        whole = jnp.concatenate([behind] * (tok // LANES), axis=1)
-        weight = jnp.exp2(neg - soft - suffix - whole)
-        if masked:
-            weight = jnp.where(seen, weight, 0.0)
-        acc[rows] += jnp.dot(weight.astype(BF16), tile, preferred_element_type=F32)
-        total = suffix[:, 0:1] + stay[:, 0:1].astype(F32)
+        acc[rows] += jnp.exp2(-behind) * jnp.dot(weight, tile, preferred_element_type=F32)
         later[rows] = behind + jnp.broadcast_to(total, (rows_group, LANES))
 
     for low_group in reversed(range(GROUPS)):
         tiles = 2 * strips
-
-        def step(i, carry, low_group=low_group, tiles=tiles):
-            j = tiles * (low_group + 1) - 1 - i
-            for g in range(low_group, GROUPS):
-                tile_step(j, g, g == low_group)
+        active = list(range(low_group, GROUPS))
+        unroll = min(tiles, 4 if len(active) == 1 else 2)
+
+        def step(i, carry, low_group=low_group, active=active, unroll=unroll):
+            tasks = [
+                (tiles * (low_group + 1) - 1 - i * unroll - u, g)
+                for u in range(unroll)
+                for g in active
+            ]
+            held = {}
+            for t in range(len(tasks) + 2):
+                if t < len(tasks):
+                    j, g = tasks[t]
+                    held[t] = chances(j, g, g == low_group)
+                if 1 <= t <= len(tasks):
+                    held[t - 1] = weights(*held[t - 1])
+                if t >= 2:
+                    gather(tasks[t - 2][1], *held.pop(t - 2))
             return carry
 
-        lax.fori_loop(0, tiles, step, 0)
-        if low_group:
-            serve(3 + GROUPS - 1 - low_group)
+        lax.fori_loop(0, tiles // unroll, step, 0)
+        if low_group != GROUPS - 1:
+            serve(3 + GROUPS - 2 - low_group)
 
     for zs in range(nz):
         rows = acc[zs * piece : (zs + 1) * piece]
@@ -288,6 +338,8 @@
         copy.start()
         ends.append(copy)
 
+    serve(6)
+
     own_wo.wait()
     for d in range(1, nx):
         got = wo.at[xat(-d), own_half]
@@ -302,7 +354,7 @@
     for d in order:
         zs = zat(-d)
         remote(mo.at[z], m2.at[zs], m2_s.at[d - 1], m2_r.at[d - 1], sp=zat(d) * 2 + c).wait_recv()
-    serve(6)
+    serve(7)
 
     top, bottom = [], []
     keep = low(half)
@@ -313,6 +365,7 @@
     mixed = jnp.concatenate(
         [jnp.concatenate(top, axis=1), jnp.concatenate(bottom, axis=1)], axis=0
     )
+    loads[6].wait()
     chunk = min(512, width)
     square = jnp.zeros((piece, 1), F32)
     for n in range(width // chunk):
@@ -345,8 +398,8 @@
         for copy in rims:
             copy.start()
 
-    serve(7)
     serve(8)
+    serve(9)
     for d in range(1, nx):
         rows = ext.at[pl.ds(pl.multiple_of(HALO + xat(-d) * piece, HALO), piece)]
         remote(rows, rows, nx_s.at[d - 1], nx_r.at[d - 1], tp=xat(d)).wait_recv()
@@ -356,9 +409,14 @@
     def _():
         ext[0:HALO] = jnp.zeros((HALO, width), BF16)
 
-    for index in range(nz):
-        there = wf.at[slab_rows(zat(-index), 1 - c)]
-        remote(there, there, wp_s.at[index], wp_r.at[index], sp=partner).wait_recv()
+    def all_across(kind):
+        for index in range(nz):
+            there = wf.at[slab_rows(zat(-index), 1 - c), lanes[kind]]
+            remote(
+                there, there, wp_s.at[kind, index], wp_r.at[kind, index], sp=partner
+            ).wait_recv()
+
+    all_across(0)
 
     chunk = min(256, ff)
 
@@ -387,6 +445,7 @@
             rsr.at[d - 1, :, cols], rs_s.at[d - 1], rs_r.at[d - 1], tp=xat(d),
         )
 
+    all_across(1)
     far_first = sorted(range(1, nx), key=lambda d: -min(d, nx - d))
     for n in range(nz // 2):
         sides = []
@@ -426,6 +485,9 @@
             s2.at[:, 0:piece], kv.at[:, c, x], s3_s.at[e - 1], s3_r.at[e - 1], tp=xat(e)
         ).wait_send()
         rs_copy(e, everything).wait_send()
+        remote(
+            wo_ref.at[own_half], wo.at[x, own_half], wo_s.at[e - 1], wo_r.at[e - 1], tp=xat(e)
+        ).wait_send()
 
     @pl.when(last_x)
     def _():
@@ -448,6 +510,12 @@
     vmem = pltpu.VMEM
     dma = pltpu.SemaphoreType.DMA
     scratch = [
+        vmem((tok, mix), BF16),
+        vmem((tok, mix), BF16),
+        vmem((tok, mix), BF16),
+        vmem((piece, width), BF16),
+        vmem((HEAD, ff // 2), BF16),
+        vmem((nz * piece, LANES), jnp.int32),
         vmem((nx, heads, packed, LANES), BF16),
         vmem((nx, heads, packed, LANES), BF16),
         vmem((nz, packed, LANES), BF16),
@@ -460,7 +528,7 @@
         vmem((nz, piece // 2, LANES), BF16),
         vmem((nx, out_weight.shape[0], width), BF16),
         vmem((2 * nz * slab, 2 * ff + blocks * LANES), BF16),
-        vmem((ff // 2, HEAD), BF16),
+        vmem((HEAD, ff // 2), BF16),
         vmem((piece, width), BF16),
         vmem((HALO + tok, width), BF16),
         vmem((tok, ff), BF16),
@@ -473,9 +541,10 @@
         dma((nz - 1,)), dma((nz - 1,)),
         dma((nx - 1,)), dma((nx - 1,)),
         dma((nx,)), dma((nx,)),
-        dma((nz // 2,)), dma((nz // 2,)),
-        dma((nz - 1 - nz // 2,)), dma((nz - 1 - nz // 2,)),
-        dma((nz,)), dma((nz,)),
+        dma((7,)),
+        dma((2, nz // 2)), dma((2, nz // 2)),
+        dma((2, nz // 2)), dma((2, nz // 2)),
+        dma((2, nz)), dma((2, nz)),
         dma, dma((nx - 1,)), dma((nx - 1,)),
         dma((nx - 1,)), dma((nx - 1,)),
         dma((nz - 1,)), dma((nz - 1,)),
@@ -485,10 +554,11 @@
         dma, dma,
     ]
     in_vmem = pl.BlockSpec(memory_space=pltpu.VMEM)
-    specs = [in_vmem] * 11
-    specs[4] = pl.BlockSpec(memory_space=pl.ANY)
+    anywhere = pl.BlockSpec(memory_space=pl.ANY)
+    specs = [anywhere] * 7 + [in_vmem] * 3 + [anywhere]
     args = list(args)
     args[9] = args[9].reshape(1, width)
+    args[10] = args[10].T
     return pl.pallas_call(
         functools.partial(kernel, dims),
         out_shape=jax.ShapeDtypeStruct((piece, width), BF16),
@@ -496,7 +566,7 @@
         out_specs=in_vmem,
         scratch_shapes=scratch + sems,
         compiler_params=pltpu.CompilerParams(
-            collective_id=0, has_side_effects=True, vmem_limit_bytes=48 * 1024 * 1024
+            collective_id=0, has_side_effects=True, vmem_limit_bytes=67043328
         ),
         name="layer",
     )(*args)

time: 160 us -> 145 us (0.906)
  Pallas kernels: 152 us -> 143 us
  local copies, waits for them, and re-layouts: 7.53 us -> 1.67 us
    pallas_call x1, Pallas kernels: 152 us -> 143 us  [body(): pl.pallas_call(functools.partial(kernel, dims), out_shape=jax.ShapeDtypeS...]
    unnamed x22 -> x1, local copies, waits for them, and re-layouts: 7.53 us -> 1.67 us
where the time goes in v2:
time: 145 us
  Pallas kernels  143 us (99%)
  local copies, waits for them, and re-layouts  1.67 us (1%)
    pallas_call x1, Pallas kernels, body(): pl.pallas_call(functools.partial(kernel, dims), out_shape=jax.ShapeDtypeS...  143 us

profile of v2, /device:TPU:33, one launch (start us, length us, event | category | flops | bytes accessed | tf_op | source)
XLA Modules:
  0.0 145.0 jit_solution(12501247533758045345)
XLA Ops:
  0.0 143.3 %layer.1 = bf16[64,2048]{1,0:T(8,128)(2,1)} custom-call(bf16[256,256]{1,0:T(8,128)(2,1)} %q_hbm.1, bf16[256,256]{1,0:T(8,128)(2,1)} %k_hbm.1, bf16[256,256]{1,0:T(8,128)(2,1)} %v_hbm.1, bf16[64,2048]{1,0:T(8,128)(2,1)} %resid_hbm.1, bf16[256,2048]{1,0:T(8,128)(2,1)} %wo_ref.1, bf16[64,768]{1,0:T(8,128)(2,1)} %gw_ref.1, bf16[64,768]{1,0:T(8,128)(2,1)} %vw_ref.1, ...), custom_call_target="tpu_custom_call" | custom-call | tf_op jit(solution)/shard_map/layer/pallas_call | solution.py:562
  143.3 1.7 %copy.13 = bf16[64,2048]{1,0:T(8,128)(2,1)} copy(bf16[64,2048]{1,0:T(8,128)(2,1)} %layer.1) | data formatting | bytes 524288

commit v3 on v2

--- a/solution.py
+++ b/solution.py
@@ -24,7 +24,7 @@
     q_hbm, k_hbm, v_hbm, resid_hbm, wo_ref, gw_ref, vw_ref, cg_ref, cv_ref, gain_ref, dw_ref,
     out_ref,
     q_ref, k_ref, v_ref, resid_ref, dwn, place, pack, s1, s2, kv, qx, tri, acc, later, mo, m2, wo, wf, dpart, state, ext, gated, rsb, pf, rsr,
-    s1_s, s1_r, s2_s, s2_r, s3_s, s3_r, sp_s, sp_r, in_l, cw_s, cw_r, cc_s, cc_r, wp_s, wp_r,
+    s1_s, s1_r, s2_s, s2_r, s3_s, s3_r, sp_s, sp_r, in_l, cw_s, cw_r, cc_s, cc_r, wp_s, wp_r, wy_s, wy_r,
     wo_l, wo_s, wo_r, wop_s, wop_r, m2_s, m2_r, nx_s, nx_r, ha_s, ha_r, rs_s, rs_r, dp_s, dp_r,
 ):
     nx, nz, heads, tok, piece, width, ff, slab = dims
@@ -38,6 +38,9 @@
     z = lax.div(sp, 2)
     c = lax.rem(sp, 2)
     partner = z * 2 + 1 - c
+    group = lax.axis_index("grp")
+    side = lax.rem(group, 2)
+    twin = group + 1 - 2 * side
     low = lambda rows: lax.broadcasted_iota(jnp.int32, (rows, LANES), 1) < HEAD
     swap = lambda a: pltpu.roll(a, HEAD, 1)
 
@@ -104,6 +107,7 @@
     for d in range(1, nz):
         greet(sp=zat(d) * 2 + c)
     greet(sp=partner)
+    greet(grp=twin)
     greet(sp=before, tp=nx - 1)
 
     @pl.when(last_x)
@@ -111,7 +115,7 @@
         for xp in range(nx):
             greet(sp=after, tp=xp)
 
-    pl.semaphore_wait(barrier, nx - 1 + nz - 1 + 2 + jnp.where(last_x, nx, 0))
+    pl.semaphore_wait(barrier, nx - 1 + nz - 1 + 3 + jnp.where(last_x, nx, 0))
 
     ends = []
     for d in range(1, nx):
@@ -159,64 +163,76 @@
             j * slab : (j + 1) * slab
         ]
     hops = (nz // 2, nz - 1 - nz // 2)
-    lanes = (slice(0, 2 * ff), slice(2 * ff, 2 * ff + blocks * LANES))
-
-    def ring(way, kind, step):
-        origin = zat(-step) if way == 0 else zat(step)
-        part = wf.at[slab_rows(origin, c), lanes[kind]]
+    lanes = (
+        pl.ds(pl.multiple_of(side * ff, LANES), ff),
+        pl.ds(2 * ff, blocks * LANES),
+        pl.ds(pl.multiple_of((1 - side) * ff, LANES), ff),
+    )
+
+    def slab_part(origin, kind, core=c):
+        return wf.at[slab_rows(origin, core), lanes[kind]]
+
+    def from_hops(way, step):
+        return zat(-step) if way == 0 else zat(step)
+
+    def ring(way, kind, step, sem):
+        part = slab_part(from_hops(way, step), kind)
         sends, recvs = ((cw_s, cw_r), (cc_s, cc_r))[way]
         to = zat(1) if way == 0 else zat(-1)
-        return remote(part, part, sends.at[kind, step], recvs.at[kind, step], sp=to * 2 + c)
-
-    def come(way, kind, step):
-        origin = zat(-step) if way == 0 else zat(step)
-        part = wf.at[slab_rows(origin, c), lanes[kind]]
-        sends, recvs = ((cw_s, cw_r), (cc_s, cc_r))[way]
-        to = zat(1) if way == 0 else zat(-1)
-        return remote(
-            part, part, sends.at[kind, step - 1], recvs.at[kind, step - 1], sp=to * 2 + c
-        )
+        return remote(part, part, sends.at[kind, sem], recvs.at[kind, sem], sp=to * 2 + c)
+
+    def across(origin, kind, index, core=c):
+        part = slab_part(origin, kind, core)
+        return remote(part, part, wp_s.at[kind, index], wp_r.at[kind, index], sp=partner)
+
+    def twin_copy(origin, index, kind=0):
+        part = slab_part(origin, kind)
+        return remote(part, part, wy_s.at[index], wy_r.at[index], grp=twin)
 
     def begin(copy):
         copy.start()
         ends.append(copy)
 
-    def send_across(origin, kind, index):
-        part = wf.at[slab_rows(origin, c), lanes[kind]]
-        begin(remote(part, part, wp_s.at[kind, index], wp_r.at[kind, index], sp=partner))
-
     for kind in range(2):
         for way in range(2):
-            begin(ring(way, kind, 0))
-    for kind in range(2):
-        send_across(z, kind, 0)
+            begin(ring(way, kind, 0, 0))
+    for kind in range(3):
+        begin(across(z, kind, 0))
 
     def serve(step):
-        for kind in range(2):
-            at = step - kind
-            for way in range(2):
-                if 1 <= at <= hops[way]:
-                    come(way, kind, at).wait_recv()
-                    if at < hops[way]:
-                        begin(ring(way, kind, at))
-                    send_across(
-                        zat(-at) if way == 0 else zat(at), kind, at if way == 0 else nz - at
-                    )
-
-    for d in range(1, nx):
+        for way in range(2):
+            if step <= hops[way]:
+                origin, index = from_hops(way, step), step if way == 0 else nz - step
+                ring(way, 0, step, step - 1).wait_recv()
+                if step < hops[way]:
+                    begin(ring(way, 0, step, step))
+                begin(twin_copy(origin, index))
+                begin(across(origin, 0, index))
+        at = step - 1
+        for way in range(2):
+            if 1 <= at <= hops[way]:
+                origin, index = from_hops(way, at), at if way == 0 else nz - at
+                ring(way, 1, at, at - 1).wait_recv()
+                if at < hops[way]:
+                    begin(ring(way, 1, at, at))
+                begin(across(origin, 1, index))
+                twin_copy(origin, index, 2).wait_recv()
+                begin(across(origin, 2, index))
+
+    order = sorted(range(1, nz), key=lambda d: (-min(d, nz - d), d))
+    for e in range(1, nx):
         remote(
-            pack.at[x], s1.at[xat(-d)], s1_s.at[d - 1], s1_r.at[d - 1], tp=xat(d)
+            pack.at[x], s1.at[xat(-e)], s1_s.at[e - 1], s1_r.at[e - 1], tp=xat(e)
         ).wait_recv()
     s2[z] = s1[lax.div(z, heads), lax.rem(z, heads)]
-    order = sorted(range(1, nz), key=lambda d: (min(d, nz - d), d))
     for d in order:
         h = zat(d)
-        copy = remote(
-            s1.at[lax.div(h, heads), lax.rem(h, heads)], s2.at[z], s2_s.at[d - 1], s2_r.at[d - 1],
-            sp=h * 2 + c,
+        begin(
+            remote(
+                s1.at[lax.div(h, heads), lax.rem(h, heads)], s2.at[z], s2_s.at[d - 1],
+                s2_r.at[d - 1], sp=h * 2 + c,
+            )
         )
-        copy.start()
-        ends.append(copy)
 
     r = lax.broadcasted_iota(jnp.int32, (tok, tok), 0)
     s = lax.broadcasted_iota(jnp.int32, (tok, tok), 1)
@@ -224,12 +240,11 @@
     row = lax.broadcasted_iota(jnp.int32, (nz * piece, LANES), 0)
     strip = lax.div(row, piece)
     place[...] = strip * (2 * tok - piece) + row + c * tok + x * piece
+    scale = LOG2E / math.sqrt(HEAD)
     acc[...] = jnp.zeros_like(acc)
     later[...] = jnp.zeros_like(later)
-    for number, d in enumerate([0] + order):
+    for d in [0] + order:
         zs = zat(-d)
-        if number < wo_parts // 2:
-            send_wo(number)
         if d:
             remote(
                 s2.at[z], s2.at[zs], s2_s.at[d - 1], s2_r.at[d - 1], sp=zat(d) * 2 + c
@@ -246,12 +261,10 @@
         qx[pl.ds(pl.multiple_of(at + half, half), half)] = jnp.where(
             keep, swap(packed), 0.0
         ).astype(BF16)
-    across = remote(
-        s2.at[:, 0:piece], kv.at[:, c, x], sp_s.at[0], sp_r.at[0], sp=partner
+    begin(
+        remote(s2.at[:, 0:piece], kv.at[:, c, x], sp_s.at[0], sp_r.at[0], sp=partner)
     )
-    across.start()
-    ends.append(across)
-    for part in range(wo_parts // 2, wo_parts):
+    for part in range(wo_parts):
         send_wo(part)
     serve(1)
     for e in (1, nx - 1) + tuple(range(2, nx - 1)) if nx > 2 else (1,):
@@ -260,23 +273,18 @@
         remote(
             s2.at[:, 0:piece], got, s3_s.at[e - 1], s3_r.at[e - 1], tp=xat(e)
         ).wait_recv()
-        across = remote(got, got, sp_s.at[e], sp_r.at[e], sp=partner)
-        across.start()
-        ends.append(across)
+        begin(remote(got, got, sp_s.at[e], sp_r.at[e], sp=partner))
     for e in range(nx):
         there = kv.at[:, 1 - c, xat(-e)]
         remote(there, there, sp_s.at[e], sp_r.at[e], sp=partner).wait_recv()
     serve(2)
 
-    scale = LOG2E / math.sqrt(HEAD)
-
-    def group_rows(g):
-        return slice(g * rows_group, (g + 1) * rows_group)
-
-    def chances(j, g, masked):
+    tiles = 2 * strips
+
+    def chances(j, rows, masked):
         tile = kv[lax.div(j, 2), lax.rem(j, 2)].reshape(tok, LANES)
         score = lax.dot_general(
-            qx[group_rows(g)], tile, (((1,), (1,)), ((), ())), preferred_element_type=F32
+            qx[rows], tile, (((1,), (1,)), ((), ())), preferred_element_type=F32
         ) * scale
         neg = jnp.minimum(score, 0.0)
         pos = jnp.maximum(score, 0.0)
@@ -284,7 +292,7 @@
         stay = pos + soft
         seen = None
         if masked:
-            where = jnp.concatenate([place[group_rows(g)]] * (tok // LANES), axis=1)
+            where = jnp.concatenate([place[rows]] * (tok // LANES), axis=1)
             seen = lax.broadcasted_iota(jnp.int32, (rows_group, tok), 1) < where - j * tok
             stay = jnp.where(seen, stay, 0.0)
         return tile, neg - soft, stay.astype(BF16), seen
@@ -296,18 +304,15 @@
             weight = jnp.where(seen, weight, 0.0)
         return tile, weight.astype(BF16), suffix[:, 0:1] + stay[:, 0:1].astype(F32)
 
-    def gather(g, tile, weight, total):
-        rows = group_rows(g)
+    def gather(rows, tile, weight, total):
         behind = later[rows]
-        acc[rows] += jnp.exp2(-behind) * jnp.dot(weight, tile, preferred_element_type=F32)
-        later[rows] = behind + jnp.broadcast_to(total, (rows_group, LANES))
-
-    for low_group in reversed(range(GROUPS)):
-        tiles = 2 * strips
-        active = list(range(low_group, GROUPS))
-        unroll = min(tiles, 4 if len(active) == 1 else 2)
-
-        def step(i, carry, low_group=low_group, active=active, unroll=unroll):
+        acc[rows] += jnp.exp2(behind) * jnp.dot(weight, tile, preferred_element_type=F32)
+        later[rows] = behind - jnp.broadcast_to(total, behind.shape)
+
+    def stretch(low_group, active, unroll):
+        unroll = min(tiles, unroll)
+
+        def step(i, carry):
             tasks = [
                 (tiles * (low_group + 1) - 1 - i * unroll - u, g)
                 for u in range(unroll)
@@ -317,28 +322,44 @@
             for t in range(len(tasks) + 2):
                 if t < len(tasks):
                     j, g = tasks[t]
-                    held[t] = chances(j, g, g == low_group)
+                    held[t] = chances(j, group_rows(g), g == low_group)
                 if 1 <= t <= len(tasks):
                     held[t - 1] = weights(*held[t - 1])
                 if t >= 2:
-                    gather(tasks[t - 2][1], *held.pop(t - 2))
+                    gather(group_rows(tasks[t - 2][1]), *held.pop(t - 2))
             return carry
 
         lax.fori_loop(0, tiles // unroll, step, 0)
-        if low_group != GROUPS - 1:
-            serve(3 + GROUPS - 2 - low_group)
-
-    for zs in range(nz):
-        rows = acc[zs * piece : (zs + 1) * piece]
-        mo[zs] = jnp.where(low(half), swap(rows[:half]), rows[half:]).astype(BF16)
-    m2[z] = mo[z]
-    for d in order:
-        h = zat(d)
-        copy = remote(mo.at[h], m2.at[z], m2_s.at[d - 1], m2_r.at[d - 1], sp=h * 2 + c)
-        copy.start()
-        ends.append(copy)
-
-    serve(6)
+
+    def group_rows(g):
+        return slice(g * rows_group, (g + 1) * rows_group)
+
+    def send_rows(g):
+        for zs in range(g * strips, (g + 1) * strips):
+            rows = acc[zs * piece : (zs + 1) * piece]
+            mo[zs] = jnp.where(low(half), swap(rows[:half]), rows[half:]).astype(BF16)
+        for zs in range(g * strips, (g + 1) * strips):
+
+            @pl.when(z == zs)
+            def _():
+                m2[zs] = mo[zs]
+
+            @pl.when(z != zs)
+            def _():
+                d = lax.rem(zs - z + nz, nz) - 1
+                remote(mo.at[zs], m2.at[z], m2_s.at[d], m2_r.at[d], sp=zs * 2 + c).start()
+
+    stretch(3, (3,), 4)
+    stretch(2, (2, 3), 2)
+    serve(3)
+    stretch(1, (1, 2, 3), 2)
+    serve(4)
+    stretch(0, (2, 3), 2)
+    send_rows(3)
+    send_rows(2)
+    stretch(0, (0, 1), 2)
+    send_rows(1)
+    send_rows(0)
 
     own_wo.wait()
     for d in range(1, nx):
@@ -347,6 +368,7 @@
         copy = remote(got, got, wop_s.at[d - 1], wop_r.at[d - 1], sp=partner)
         copy.start()
         ends.append(copy)
+    serve(5)
     other_half = pl.ds(pl.multiple_of((1 - c) * share, share), share)
     for d in range(1, nx):
         there = wo.at[xat(-d), other_half]
@@ -354,7 +376,7 @@
     for d in order:
         zs = zat(-d)
         remote(mo.at[z], m2.at[zs], m2_s.at[d - 1], m2_r.at[d - 1], sp=zat(d) * 2 + c).wait_recv()
-    serve(7)
+    serve(6)
 
     top, bottom = [], []
     keep = low(half)
@@ -398,6 +420,7 @@
         for copy in rims:
             copy.start()
 
+    serve(7)
     serve(8)
     serve(9)
     for d in range(1, nx):
@@ -411,12 +434,10 @@
 
     def all_across(kind):
         for index in range(nz):
-            there = wf.at[slab_rows(zat(-index), 1 - c), lanes[kind]]
-            remote(
-                there, there, wp_s.at[kind, index], wp_r.at[kind, index], sp=partner
-            ).wait_recv()
+            across(zat(-index), kind, index, 1 - c).wait_recv()
 
     all_across(0)
+    all_across(2)
 
     chunk = min(256, ff)
 
@@ -480,6 +501,8 @@
 
     for copy in ends:
         copy.wait_send()
+    for d in range(1, nz):
+        remote(mo.at[zat(d)], m2.at[z], m2_s.at[d - 1], m2_r.at[d - 1], sp=zat(d) * 2 + c).wait_send()
     for e in range(1, nx):
         remote(
             s2.at[:, 0:piece], kv.at[:, c, x], s3_s.at[e - 1], s3_r.at[e - 1], tp=xat(e)
@@ -544,7 +567,8 @@
         dma((7,)),
         dma((2, nz // 2)), dma((2, nz // 2)),
         dma((2, nz // 2)), dma((2, nz // 2)),
-        dma((2, nz)), dma((2, nz)),
+        dma((3, nz)), dma((3, nz)),
+        dma((nz,)), dma((nz,)),
         dma, dma((nx - 1,)), dma((nx - 1,)),
         dma((nx - 1,)), dma((nx - 1,)),
         dma((nz - 1,)), dma((nz - 1,)),
@@ -566,7 +590,7 @@
         out_specs=in_vmem,
         scratch_shapes=scratch + sems,
         compiler_params=pltpu.CompilerParams(
-            collective_id=0, has_side_effects=True, vmem_limit_bytes=67043328
+            collective_id=0, has_side_effects=True, vmem_limit_bytes=66 * 1000 * 1000
         ),
         name="layer",
     )(*args)

time: 145 us -> 135 us (0.931)
  Pallas kernels: 143 us -> 134 us
    pallas_call x1, Pallas kernels: 143 us -> 134 us  [body(): pl.pallas_call(functools.partial(kernel, dims), out_shape=jax.ShapeDtypeS...]
where the time goes in v3:
time: 135 us
  Pallas kernels  134 us (99%)
  local copies, waits for them, and re-layouts  1.67 us (1%)
    pallas_call x1, Pallas kernels, body(): pl.pallas_call(functools.partial(kernel, dims), out_shape=jax.ShapeDtypeS...  134 us

profile of v3, /device:TPU:33, one launch (start us, length us, event | category | flops | bytes accessed | tf_op | source)
XLA Modules:
  0.0 135.2 jit_solution(11528944417008072127)
XLA Ops:
  0.0 133.5 %layer.1 = bf16[64,2048]{1,0:T(8,128)(2,1)} custom-call(bf16[256,256]{1,0:T(8,128)(2,1)} %q_hbm.1, bf16[256,256]{1,0:T(8,128)(2,1)} %k_hbm.1, bf16[256,256]{1,0:T(8,128)(2,1)} %v_hbm.1, bf16[64,2048]{1,0:T(8,128)(2,1)} %resid_hbm.1, bf16[256,2048]{1,0:T(8,128)(2,1)} %wo_ref.1, bf16[64,768]{1,0:T(8,128)(2,1)} %gw_ref.1, bf16[64,768]{1,0:T(8,128)(2,1)} %vw_ref.1, ...), custom_call_target="tpu_custom_call" | custom-call | tf_op jit(solution)/shard_map/layer/pallas_call | solution.py:586
  133.6 1.7 %copy.13 = bf16[64,2048]{1,0:T(8,128)(2,1)} copy(bf16[64,2048]{1,0:T(8,128)(2,1)} %layer.1) | data formatting | bytes 524288

commit v4 on v3

--- a/solution.py
+++ b/solution.py
@@ -274,10 +274,10 @@
             s2.at[:, 0:piece], got, s3_s.at[e - 1], s3_r.at[e - 1], tp=xat(e)
         ).wait_recv()
         begin(remote(got, got, sp_s.at[e], sp_r.at[e], sp=partner))
+    serve(2)
     for e in range(nx):
         there = kv.at[:, 1 - c, xat(-e)]
         remote(there, there, sp_s.at[e], sp_r.at[e], sp=partner).wait_recv()
-    serve(2)
 
     tiles = 2 * strips
 
@@ -350,13 +350,15 @@
                 remote(mo.at[zs], m2.at[z], m2_s.at[d], m2_r.at[d], sp=zs * 2 + c).start()
 
     stretch(3, (3,), 4)
+    serve(3)
     stretch(2, (2, 3), 2)
-    serve(3)
+    serve(4)
     stretch(1, (1, 2, 3), 2)
-    serve(4)
+    serve(5)
     stretch(0, (2, 3), 2)
     send_rows(3)
     send_rows(2)
+    serve(6)
     stretch(0, (0, 1), 2)
     send_rows(1)
     send_rows(0)
@@ -368,7 +370,7 @@
         copy = remote(got, got, wop_s.at[d - 1], wop_r.at[d - 1], sp=partner)
         copy.start()
         ends.append(copy)
-    serve(5)
+    serve(7)
     other_half = pl.ds(pl.multiple_of((1 - c) * share, share), share)
     for d in range(1, nx):
         there = wo.at[xat(-d), other_half]
@@ -376,7 +378,7 @@
     for d in order:
         zs = zat(-d)
         remote(mo.at[z], m2.at[zs], m2_s.at[d - 1], m2_r.at[d - 1], sp=zat(d) * 2 + c).wait_recv()
-    serve(6)
+    serve(8)
 
     top, bottom = [], []
     keep = low(half)
@@ -404,11 +406,23 @@
     mine_rows = pl.ds(pl.multiple_of(HALO + x * piece, HALO), piece)
     ext[mine_rows] = (state[...].astype(F32) * factor * gain_ref[...]).astype(BF16)
 
-    for d in range(1, nx):
-        rows = ext.at[mine_rows]
-        copy = remote(rows, rows, nx_s.at[d - 1], nx_r.at[d - 1], tp=xat(d))
-        copy.start()
-        ends.append(copy)
+    sides = (xat(1), xat(-1))
+    halves = (slice(0, width // 2), slice(width // 2, width))
+
+    def normed_half(origin, h):
+        return ext.at[pl.ds(pl.multiple_of(HALO + origin * piece, HALO), piece), halves[h]]
+
+    def normed_copy(way, h, origin):
+        part = normed_half(origin, h)
+        return remote(part, part, nx_s.at[way, h], nx_r.at[way, h], tp=sides[way])
+
+    def normed_on(way, origin):
+        part = normed_half(origin, way)
+        return remote(part, part, nx_s.at[way, 2], nx_r.at[way, 2], tp=sides[way])
+
+    for turn_h in range(2):
+        for way in range(2):
+            begin(normed_copy(way, turn_h if way == 0 else 1 - turn_h, x))
 
     rim = ext.at[nx * piece : nx * piece + HALO]
     rims = [
@@ -420,12 +434,14 @@
         for copy in rims:
             copy.start()
 
-    serve(7)
-    serve(8)
+    for way in range(2):
+        normed_copy(way, way, sides[1 - way]).wait_recv()
+        begin(normed_on(way, sides[1 - way]))
     serve(9)
-    for d in range(1, nx):
-        rows = ext.at[pl.ds(pl.multiple_of(HALO + xat(-d) * piece, HALO), piece)]
-        remote(rows, rows, nx_s.at[d - 1], nx_r.at[d - 1], tp=xat(d)).wait_recv()
+    for way in range(2):
+        normed_copy(way, 1 - way, sides[1 - way]).wait_recv()
+    for way in range(2):
+        normed_on(way, xat(2)).wait_recv()
     rims[0].wait_recv()
 
     @pl.when(sp == 0)
@@ -460,18 +476,23 @@
         value = conv(value, cv_ref, cols)
         gated[:, cols] = (gate / (1.0 + jnp.exp(-gate)) * value).astype(BF16)
 
-    def rs_copy(d, cols):
+    def block_rows(at):
+        return pl.ds(pl.multiple_of(at * piece, piece), piece)
+
+    def sum_copy(way, stage, cols):
+        at = xat(2) if stage == 0 else sides[way]
+        slot = 2 if stage == 0 else way
         return remote(
-            rsb.at[pl.ds(pl.multiple_of(xat(d) * piece, piece), piece), cols],
-            rsr.at[d - 1, :, cols], rs_s.at[d - 1], rs_r.at[d - 1], tp=xat(d),
+            rsb.at[block_rows(at), cols], rsr.at[slot, :, cols], rs_s.at[way, stage],
+            rs_r.at[way, stage], tp=sides[way],
         )
 
     all_across(1)
-    far_first = sorted(range(1, nx), key=lambda d: -min(d, nx - d))
-    for n in range(nz // 2):
-        sides = []
+    quarter = nz // 4
+    for n in [h * quarter + i for i in range(quarter) for h in range(2)]:
+        pair = []
         for zz in (2 * n, 2 * n + 1):
-            sides.append(
+            pair.append(
                 jnp.concatenate(
                     [
                         wf[
@@ -485,29 +506,39 @@
                 )
             )
         part = jnp.dot(
-            gated[...], jnp.concatenate(sides, axis=1), preferred_element_type=F32
+            gated[...], jnp.concatenate(pair, axis=1), preferred_element_type=F32
         )
         cols = slice(n * 2 * LANES, (n + 1) * 2 * LANES)
         pf[:, cols] = part
         rsb[:, cols] = part.astype(BF16)
-        for d in far_first:
-            rs_copy(d, cols).start()
-    everything = slice(0, width)
-    total = state[...].astype(F32) + pf[pl.ds(pl.multiple_of(x * piece, piece), piece)]
-    for d in range(1, nx):
-        rs_copy(d, everything).wait_recv()
-        total = total + rsr[d - 1].astype(F32)
-    out_ref[...] = total.astype(BF16)
+        sum_copy(n // quarter, 0, cols).start()
+    for way in range(2):
+        begin(sum_copy(way, 1, halves[1 - way]))
+    for way in range(2):
+        cols = halves[way]
+        sum_copy(way, 0, cols).wait_recv()
+        rsb[block_rows(sides[way]), cols] = (
+            pf[block_rows(sides[way]), cols] + rsr[2, :, cols].astype(F32)
+        ).astype(BF16)
+        begin(sum_copy(way, 2, cols))
+    for h in range(2):
+        cols = halves[h]
+        sum_copy(1 - h, 1, cols).wait_recv()
+        sum_copy(h, 2, cols).wait_recv()
+        total = state[:, cols].astype(F32) + pf[block_rows(x), cols]
+        total = total + rsr[0, :, cols].astype(F32) + rsr[1, :, cols].astype(F32)
+        out_ref[:, cols] = total.astype(BF16)
 
     for copy in ends:
         copy.wait_send()
+    for way in range(2):
+        sum_copy(way, 0, halves[way]).wait_send()
     for d in range(1, nz):
         remote(mo.at[zat(d)], m2.at[z], m2_s.at[d - 1], m2_r.at[d - 1], sp=zat(d) * 2 + c).wait_send()
     for e in range(1, nx):
         remote(
             s2.at[:, 0:piece], kv.at[:, c, x], s3_s.at[e - 1], s3_r.at[e - 1], tp=xat(e)
         ).wait_send()
-        rs_copy(e, everything).wait_send()
         remote(
             wo_ref.at[own_half], wo.at[x, own_half], wo_s.at[e - 1], wo_r.at[e - 1], tp=xat(e)
         ).wait_send()
@@ -526,7 +557,7 @@
     ff = gate_weight.shape[1]
     slab = gate_weight.shape[0]
     heads = mix // HEAD
-    assert heads * nx == nz
+    assert heads * nx == nz and nx == 4
     blocks = ff // 2 // slab
     dims = (nx, nz, heads, tok, piece, width, ff, slab)
     packed = piece + piece // 2
@@ -572,9 +603,9 @@
         dma, dma((nx - 1,)), dma((nx - 1,)),
         dma((nx - 1,)), dma((nx - 1,)),
         dma((nz - 1,)), dma((nz - 1,)),
-        dma((nx - 1,)), dma((nx - 1,)),
+        dma((2, 3)), dma((2, 3)),
         dma((nx,)), dma,
-        dma((nx - 1,)), dma((nx - 1,)),
+        dma((2, 3)), dma((2, 3)),
         dma, dma,
     ]
     in_vmem = pl.BlockSpec(memory_space=pltpu.VMEM)

time: 135 us -> 132 us (0.978)
  Pallas kernels: 134 us -> 130 us
    pallas_call x1, Pallas kernels: 134 us -> 130 us  [body(): pl.pallas_call(functools.partial(kernel, dims), out_shape=jax.ShapeDtypeS...]
where the time goes in v4:
time: 132 us; the launch traced here: 131 us
  Pallas kernels  130 us (98%)
  local copies, waits for them, and re-layouts  1.67 us (1%)
    pallas_call x1, Pallas kernels, body(): pl.pallas_call(functools.partial(kernel, dims), out_shape=jax.ShapeDtypeS...  130 us

profile of v4, /device:TPU:33, one launch (start us, length us, event | category | flops | bytes accessed | tf_op | source)
XLA Modules:
  0.0 131.2 jit_solution(13583968452021715968)
XLA Ops:
  0.0 129.5 %layer.1 = bf16[64,2048]{1,0:T(8,128)(2,1)} custom-call(bf16[256,256]{1,0:T(8,128)(2,1)} %q_hbm.1, bf16[256,256]{1,0:T(8,128)(2,1)} %k_hbm.1, bf16[256,256]{1,0:T(8,128)(2,1)} %v_hbm.1, bf16[64,2048]{1,0:T(8,128)(2,1)} %resid_hbm.1, bf16[256,2048]{1,0:T(8,128)(2,1)} %wo_ref.1, bf16[64,768]{1,0:T(8,128)(2,1)} %gw_ref.1, bf16[64,768]{1,0:T(8,128)(2,1)} %vw_ref.1, ...), custom_call_target="tpu_custom_call" | custom-call | tf_op jit(solution)/shard_map/layer/pallas_call | solution.py:617
  129.5 1.7 %copy.13 = bf16[64,2048]{1,0:T(8,128)(2,1)} copy(bf16[64,2048]{1,0:T(8,128)(2,1)} %layer.1) | data formatting | bytes 524288

commit v5 on v4

--- a/solution.py
+++ b/solution.py
@@ -219,20 +219,29 @@
                 twin_copy(origin, index, 2).wait_recv()
                 begin(across(origin, 2, index))
 
-    order = sorted(range(1, nz), key=lambda d: (-min(d, nz - d), d))
+    order = sorted(range(1, nz), key=lambda d: (min(d, nz - d), d))
     for e in range(1, nx):
         remote(
             pack.at[x], s1.at[xat(-e)], s1_s.at[e - 1], s1_r.at[e - 1], tp=xat(e)
         ).wait_recv()
     s2[z] = s1[lax.div(z, heads), lax.rem(z, heads)]
-    for d in order:
-        h = zat(d)
-        begin(
-            remote(
-                s1.at[lax.div(h, heads), lax.rem(h, heads)], s2.at[z], s2_s.at[d - 1],
-                s2_r.at[d - 1], sp=h * 2 + c,
+    spans = (slice(0, piece), slice(piece, piece + half))
+    for kind in range(2):
+        for d in order:
+            h = zat(d)
+            begin(
+                remote(
+                    s1.at[lax.div(h, heads), lax.rem(h, heads), spans[kind]],
+                    s2.at[z, spans[kind]], s2_s.at[kind, d - 1], s2_r.at[kind, d - 1],
+                    sp=h * 2 + c,
+                )
             )
-        )
+
+    def arrived(kind, d):
+        part = s2.at[zat(-d), spans[kind]]
+        remote(
+            part, part, s2_s.at[kind, d - 1], s2_r.at[kind, d - 1], sp=zat(d) * 2 + c
+        ).wait_recv()
 
     r = lax.broadcasted_iota(jnp.int32, (tok, tok), 0)
     s = lax.broadcasted_iota(jnp.int32, (tok, tok), 1)
@@ -246,21 +255,12 @@
     for d in [0] + order:
         zs = zat(-d)
         if d:
-            remote(
-                s2.at[z], s2.at[zs], s2_s.at[d - 1], s2_r.at[d - 1], sp=zat(d) * 2 + c
-            ).wait_recv()
+            arrived(0, d)
         kv[zs, c, x] = s2[zs, 0:piece]
         for e in range(1, nx):
             remote(
                 s2.at[zs, 0:piece], kv.at[zs, c, x], s3_s.at[e - 1], s3_r.at[e - 1], tp=xat(e)
             ).start()
-        packed = s2[zs, piece:].astype(F32)
-        keep = low(half)
-        at = pl.multiple_of(zs * piece, piece)
-        qx[pl.ds(at, half)] = jnp.where(keep, packed, 0.0).astype(BF16)
-        qx[pl.ds(pl.multiple_of(at + half, half), half)] = jnp.where(
-            keep, swap(packed), 0.0
-        ).astype(BF16)
     begin(
         remote(s2.at[:, 0:piece], kv.at[:, c, x], sp_s.at[0], sp_r.at[0], sp=partner)
     )
@@ -275,6 +275,17 @@
         ).wait_recv()
         begin(remote(got, got, sp_s.at[e], sp_r.at[e], sp=partner))
     serve(2)
+    for d in [0] + order:
+        zs = zat(-d)
+        if d:
+            arrived(1, d)
+        packed = s2[zs, piece:].astype(F32)
+        keep = low(half)
+        at = pl.multiple_of(zs * piece, piece)
+        qx[pl.ds(at, half)] = jnp.where(keep, packed, 0.0).astype(BF16)
+        qx[pl.ds(pl.multiple_of(at + half, half), half)] = jnp.where(
+            keep, swap(packed), 0.0
+        ).astype(BF16)
     for e in range(nx):
         there = kv.at[:, 1 - c, xat(-e)]
         remote(there, there, sp_s.at[e], sp_r.at[e], sp=partner).wait_recv()
@@ -350,15 +361,14 @@
                 remote(mo.at[zs], m2.at[z], m2_s.at[d], m2_r.at[d], sp=zs * 2 + c).start()
 
     stretch(3, (3,), 4)
+    stretch(2, (2, 3), 2)
     serve(3)
-    stretch(2, (2, 3), 2)
+    stretch(1, (1, 2, 3), 2)
     serve(4)
-    stretch(1, (1, 2, 3), 2)
-    serve(5)
     stretch(0, (2, 3), 2)
     send_rows(3)
     send_rows(2)
-    serve(6)
+    serve(5)
     stretch(0, (0, 1), 2)
     send_rows(1)
     send_rows(0)
@@ -370,7 +380,7 @@
         copy = remote(got, got, wop_s.at[d - 1], wop_r.at[d - 1], sp=partner)
         copy.start()
         ends.append(copy)
-    serve(7)
+    serve(6)
     other_half = pl.ds(pl.multiple_of((1 - c) * share, share), share)
     for d in range(1, nx):
         there = wo.at[xat(-d), other_half]
@@ -378,7 +388,7 @@
     for d in order:
         zs = zat(-d)
         remote(mo.at[z], m2.at[zs], m2_s.at[d - 1], m2_r.at[d - 1], sp=zat(d) * 2 + c).wait_recv()
-    serve(8)
+    serve(7)
 
     top, bottom = [], []
     keep = low(half)
@@ -437,6 +447,7 @@
     for way in range(2):
         normed_copy(way, way, sides[1 - way]).wait_recv()
         begin(normed_on(way, sides[1 - way]))
+    serve(8)
     serve(9)
     for way in range(2):
         normed_copy(way, 1 - way, sides[1 - way]).wait_recv()
@@ -592,7 +603,7 @@
     ]
     sems = [
         dma((nx - 1,)), dma((nx - 1,)),
-        dma((nz - 1,)), dma((nz - 1,)),
+        dma((2, nz - 1)), dma((2, nz - 1)),
         dma((nx - 1,)), dma((nx - 1,)),
         dma((nx,)), dma((nx,)),
         dma((7,)),

time: 132 us -> 129 us (0.977)
  Pallas kernels: 130 us -> 127 us
    pallas_call x1, Pallas kernels: 130 us -> 127 us  [body(): pl.pallas_call(functools.partial(kernel, dims), out_shape=jax.ShapeDtypeS...]
where the time goes in v5:
time: 129 us; the launch traced here: 128 us
  Pallas kernels  127 us (98%)
  local copies, waits for them, and re-layouts  1.67 us (1%)
    pallas_call x1, Pallas kernels, body(): pl.pallas_call(functools.partial(kernel, dims), out_shape=jax.ShapeDtypeS...  127 us

profile of v5, /device:TPU:33, one launch (start us, length us, event | category | flops | bytes accessed | tf_op | source)
XLA Modules:
  0.0 128.2 jit_solution(13359924956122506620)
XLA Ops:
  0.0 126.5 %layer.1 = bf16[64,2048]{1,0:T(8,128)(2,1)} custom-call(bf16[256,256]{1,0:T(8,128)(2,1)} %q_hbm.1, bf16[256,256]{1,0:T(8,128)(2,1)} %k_hbm.1, bf16[256,256]{1,0:T(8,128)(2,1)} %v_hbm.1, bf16[64,2048]{1,0:T(8,128)(2,1)} %resid_hbm.1, bf16[256,2048]{1,0:T(8,128)(2,1)} %wo_ref.1, bf16[64,768]{1,0:T(8,128)(2,1)} %gw_ref.1, bf16[64,768]{1,0:T(8,128)(2,1)} %vw_ref.1, ...), custom_call_target="tpu_custom_call" | custom-call | tf_op jit(solution)/shard_map/layer/pallas_call | solution.py:628
  126.5 1.7 %copy.13 = bf16[64,2048]{1,0:T(8,128)(2,1)} copy(bf16[64,2048]{1,0:T(8,128)(2,1)} %layer.1) | data formatting | bytes 524288

commit v6 on v5

--- a/solution.py
+++ b/solution.py
@@ -117,11 +117,21 @@
 
     pl.semaphore_wait(barrier, nx - 1 + nz - 1 + 3 + jnp.where(last_x, nx, 0))
 
+    spans = (slice(0, piece), slice(piece, piece + half))
     ends = []
-    for d in range(1, nx):
-        copy = remote(pack.at[xat(d)], s1.at[x], s1_s.at[d - 1], s1_r.at[d - 1], tp=xat(d))
+
+    def begin(copy):
         copy.start()
         ends.append(copy)
+
+    for kind in range(2):
+        for d in range(1, nx):
+            begin(
+                remote(
+                    pack.at[xat(d), :, spans[kind]], s1.at[x, :, spans[kind]],
+                    s1_s.at[kind, d - 1], s1_r.at[kind, d - 1], tp=xat(d),
+                )
+            )
     down_part = remote(
         dw_ref.at[:, pl.ds(pl.multiple_of((1 - c) * down_rows, LANES), down_rows)], dpart, dp_s,
         dp_r, sp=partner,
@@ -189,10 +199,6 @@
         part = slab_part(origin, kind)
         return remote(part, part, wy_s.at[index], wy_r.at[index], grp=twin)
 
-    def begin(copy):
-        copy.start()
-        ends.append(copy)
-
     for kind in range(2):
         for way in range(2):
             begin(ring(way, kind, 0, 0))
@@ -220,13 +226,11 @@
                 begin(across(origin, 2, index))
 
     order = sorted(range(1, nz), key=lambda d: (min(d, nz - d), d))
-    for e in range(1, nx):
-        remote(
-            pack.at[x], s1.at[xat(-e)], s1_s.at[e - 1], s1_r.at[e - 1], tp=xat(e)
-        ).wait_recv()
-    s2[z] = s1[lax.div(z, heads), lax.rem(z, heads)]
-    spans = (slice(0, piece), slice(piece, piece + half))
     for kind in range(2):
+        for e in range(1, nx):
+            part = s1.at[xat(-e), :, spans[kind]]
+            remote(part, part, s1_s.at[kind, e - 1], s1_r.at[kind, e - 1], tp=xat(e)).wait_recv()
+        s2[z, spans[kind]] = s1[lax.div(z, heads), lax.rem(z, heads), spans[kind]]
         for d in order:
             h = zat(d)
             begin(
@@ -444,10 +448,10 @@
         for copy in rims:
             copy.start()
 
+    serve(8)
     for way in range(2):
         normed_copy(way, way, sides[1 - way]).wait_recv()
         begin(normed_on(way, sides[1 - way]))
-    serve(8)
     serve(9)
     for way in range(2):
         normed_copy(way, 1 - way, sides[1 - way]).wait_recv()
@@ -602,7 +606,7 @@
         vmem((nx - 1, piece, width), BF16),
     ]
     sems = [
-        dma((nx - 1,)), dma((nx - 1,)),
+        dma((2, nx - 1)), dma((2, nx - 1)),
         dma((2, nz - 1)), dma((2, nz - 1)),
         dma((nx - 1,)), dma((nx - 1,)),
         dma((nx,)), dma((nx,)),

time: 129 us -> 128 us (level)
  no operation moved by 1% of the time
where the time goes in v6:
time: 128 us; the launch traced here: 127 us
  Pallas kernels  126 us (98%)
  local copies, waits for them, and re-layouts  1.67 us (1%)
    pallas_call x1, Pallas kernels, body(): pl.pallas_call(functools.partial(kernel, dims), out_shape=jax.ShapeDtypeS...  126 us

profile of v6, /device:TPU:33, one launch (start us, length us, event | category | flops | bytes accessed | tf_op | source)
XLA Modules:
  0.0 127.2 jit_solution(1433546746763629802)
XLA Ops:
  0.0 125.5 %layer.1 = bf16[64,2048]{1,0:T(8,128)(2,1)} custom-call(bf16[256,256]{1,0:T(8,128)(2,1)} %q_hbm.1, bf16[256,256]{1,0:T(8,128)(2,1)} %k_hbm.1, bf16[256,256]{1,0:T(8,128)(2,1)} %v_hbm.1, bf16[64,2048]{1,0:T(8,128)(2,1)} %resid_hbm.1, bf16[256,2048]{1,0:T(8,128)(2,1)} %wo_ref.1, bf16[64,768]{1,0:T(8,128)(2,1)} %gw_ref.1, bf16[64,768]{1,0:T(8,128)(2,1)} %vw_ref.1, ...), custom_call_target="tpu_custom_call" | custom-call | tf_op jit(solution)/shard_map/layer/pallas_call | solution.py:632
  125.5 1.7 %copy.13 = bf16[64,2048]{1,0:T(8,128)(2,1)} copy(bf16[64,2048]{1,0:T(8,128)(2,1)} %layer.1) | data formatting | bytes 524288
